TPU v7x, 512 devices: a whole 4x4x16 slice. The times are simulated.
512 devices in a mesh: sp: 64 (over z, y), tp: 8 (over x, core).
Axes of the slice: x: 4, y: 4, z: 16, core: 2. Of those that a mesh axis runs over, the one named last changes fastest.
Arguments:
- tokens_in: bfloat16 [8192, 2048], P(('sp', 'tp')), may hold values from -9 to 9, as said below
- w_query: bfloat16 [2048, 2048], P(None, 'tp'), may hold values from -0.125 to 0.125
- w_key: bfloat16 [2048, 512], P(None, 'tp'), may hold values from -0.125 to 0.125
- w_value: bfloat16 [2048, 512], P(None, 'tp'), may hold values from -0.125 to 0.125
- w_out: bfloat16 [2048, 2048], P('tp'), may hold values from -0.125 to 0.125
- q_gain: float32 [64], replicated, may hold values from 0.1 to 14
- k_gain: float32 [64], replicated, may hold values from 0.1 to 14
Outputs:
- attended: bfloat16 [8192, 2048], P(('sp', 'tp'))
Inputs may be any that keep to these rules, and one draw needn't show every extreme that they name: `tokens_in`: activations whose mean differs from one block of 128 tokens to another.
All inputs are finite; a program needn't handle non-finite values.
Results may differ from a plain program's by a relative error of at most 0.014.
The roundings to bfloat16 on the way count: a program that leaves them out, or rounds other values in their place, can miss the bound.
Values may be sent and summed in bfloat16 or wider, within the bound.
No kernel may reach another device: no remote copies, remote signals or barrier semaphores. Data moves between devices by JAX's collectives and lax.ppermute only.
A program may use at most 64 MiB of HBM per device.

v0:
```python
import jax
import jax.numpy as jnp
from jax import lax
from jax.sharding import Mesh
from jax.sharding import PartitionSpec as P

GRID_W = 64
SP = ("sp_0", "sp_1")
SP_TP = ("sp_0", "sp_1", "tp")


def sent_to_all(shard, axis):
    length = lax.axis_size(axis)
    return lax.all_to_all(
        jnp.broadcast_to(shard[None], (length, *shard.shape)), axis, 0, 0, tiled=True
    )


def joined_along(blocks, dim):
    lengths = list(blocks.shape[1:])
    lengths[dim] *= blocks.shape[0]
    return jnp.moveaxis(blocks, 0, dim).reshape(lengths)


def collect(shard, axis, dim):
    blocks = sent_to_all(shard, axis)
    return joined_along(blocks, dim)


def whole_of(shard, axes, dim):
    if not axes:
        return shard
    nearer = lax.all_gather(shard, axes[-1], axis=dim, tiled=True)
    return whole_of(nearer, axes[:-1], dim)


def in_blocks(shard, dim, length):
    before, after = (shard.shape[:dim], shard.shape[dim + 1 :])
    return jnp.moveaxis(shard.reshape(*before, length, -1, *after), dim, 0)


def summed_on_arrival(shard, axis, dim):
    blocks = in_blocks(shard, dim, lax.axis_size(axis))
    arrived = lax.all_to_all(blocks, axis, split_axis=0, concat_axis=0, tiled=True)
    return arrived.astype(jnp.float32).sum(axis=0)


def turned(vectors, position, gain):
    pairs = vectors.shape[-1] // 4
    scaled = vectors * lax.rsqrt(jnp.mean(vectors * vectors, axis=-1, keepdims=True) + 1e-06) * gain
    freq = 10000.0 ** (-jnp.arange(pairs, dtype=jnp.float32) / pairs)
    grid_row = (position // GRID_W).astype(jnp.float32)
    grid_col = (position % GRID_W).astype(jnp.float32)
    angle = jnp.stack([grid_row[:, None] * freq, grid_col[:, None] * freq], axis=1)
    cosine = jnp.cos(angle)[:, None]
    sine = jnp.sin(angle)[:, None]
    split = scaled.reshape(scaled.shape[:-1] + (2, 2, pairs))
    first = split[..., 0, :]
    second = split[..., 1, :]
    joined = jnp.stack([first * cosine - second * sine, first * sine + second * cosine], axis=-2)
    return joined.reshape(scaled.shape)


def body(tokens_in, w_query, w_key, w_value, w_out, q_gain, k_gain):
    head_dim = q_gain.shape[0]
    query_cols = w_query.shape[1]
    key_cols = w_key.shape[1]
    kv_heads = key_cols // head_dim
    group = query_cols // key_cols
    w_joined = jnp.concatenate([w_query, w_key, w_value], axis=1)
    projected = jnp.dot(
        collect(tokens_in, "tp", 0), w_joined, preferred_element_type=jnp.float32
    ).astype(jnp.bfloat16)
    row_count = projected.shape[0]
    position = lax.axis_index(SP) * row_count + jnp.arange(row_count, dtype=jnp.int32)
    query_n = turned(
        projected[:, :query_cols]
        .astype(jnp.float32)
        .reshape(row_count, kv_heads * group, head_dim),
        position,
        q_gain,
    ).astype(jnp.bfloat16)
    query_g = query_n.reshape(row_count, kv_heads, group, head_dim).transpose(1, 2, 0, 3)
    raw_keys = projected[:, query_cols : query_cols + key_cols]
    values = projected[:, query_cols + key_cols :]
    scale = head_dim ** (-0.5)
    outgoing = jnp.concatenate([raw_keys, values], axis=1)
    piece = whole_of(outgoing, SP, 0)
    length = piece.shape[0]
    spot = jnp.arange(length, dtype=jnp.int32)
    keys_n = turned(
        piece[:, :key_cols].astype(jnp.float32).reshape(length, kv_heads, head_dim), spot, k_gain
    ).astype(jnp.bfloat16)
    peak = jnp.full((kv_heads, group, row_count), -1e30, jnp.float32)
    scores = (
        jnp.einsum("kgqd,nkd->kgqn", query_g, keys_n, preferred_element_type=jnp.float32) * scale
    )
    new_peak = jnp.maximum(peak, jnp.max(scores, axis=-1))
    expo = jnp.exp(scores - new_peak[..., None])
    total = jnp.sum(expo, axis=-1)
    summed = jnp.einsum(
        "kgqn,nkd->kgqd",
        expo.astype(jnp.bfloat16),
        piece[:, key_cols:].reshape(length, kv_heads, head_dim),
        preferred_element_type=jnp.float32,
    )
    peak, total, summed = (new_peak, total, summed)
    mixed = (summed / total[..., None]).astype(jnp.bfloat16)
    mixed = mixed.transpose(2, 0, 1, 3).reshape(row_count, query_cols)
    attended = summed_on_arrival(
        jnp.dot(mixed, w_out, preferred_element_type=jnp.float32).astype(jnp.bfloat16), "tp", 0
    )
    return attended.astype(jnp.bfloat16)


def solution(mesh):
    finer = Mesh(mesh.devices.reshape(16, 4, mesh.shape["tp"]), ("sp_0", "sp_1", "tp"))
    return jax.shard_map(
        body,
        mesh=finer,
        in_specs=(
            P(SP_TP, None),
            P(None, "tp"),
            P(None, "tp"),
            P(None, "tp"),
            P("tp", None),
            P(),
            P(),
        ),
        out_specs=P(SP_TP, None),
        check_vma=False,
    )
```

profile of v0, /device:TPU:1, one launch (start us, length us, event | category | flops | bytes accessed | tf_op | source)
XLA Modules:
  0.0 166.0 jit_solution(3038600253206438387)
XLA Ops:
  6.5 1.8 %broadcast_in_dim.4 = bf16[8,16,2048]{2,1,0:T(8,128)(2,1)} broadcast(bf16[16,2048]{1,0:T(8,128)(2,1)} %param.7), dimensions={1,2} | broadcast | bytes 589824 | tf_op jit(solution)/shard_map/broadcast_in_dim | solution.py:15
  8.3 10.2 %all-to-all-start = ((bf16[8,16,2048]{2,1,0:T(8,128)(2,1)}), bf16[8,16,2048]{2,1,0:T(8,128)(2,1)S(1)}, u32[]{:S(2)}, u32[]{:S(2)}) async-start(bf16[8,16,2048]{2,1,0:T(8,128)(2,1)} %broadcast_in_dim.4), calls=%async_computation | async-start | bytes 1048576 | tf_op jit(solution)/shard_map/all_to_all | solution.py:14
  18.5 1.2 copy.8
  19.8 1.2 copy.9
  21.1 6.9 %all-to-all-done = bf16[8,16,2048]{2,1,0:T(8,128)(2,1)S(1)} async-done(((bf16[8,16,2048]{2,1,0:T(8,128)(2,1)}), bf16[8,16,2048]{2,1,0:T(8,128)(2,1)S(1)}, u32[]{:S(2)}, u32[]{:S(2)}) %all-to-all-start) | async-done | bytes 524320 | tf_op jit(solution)/shard_map/all_to_all | solution.py:14
  27.9 2.1 %fusion.15 = bf16[128,384]{0,1:T(8,128)(2,1)S(1)} fusion(bf16[128,2048]{1,0:T(8,128)(2,1)S(1)} %bitcast.36, bf16[2048,64]{1,0:T(8,128)(2,1)S(1)} %copy.9, bf16[2048,64]{1,0:T(8,128)(2,1)S(1)} %copy.8, bf16[2048,256]{1,0:T(8,128)(2,1)} %param.8), kind=kOutput, calls=%fused_computation.17 | convolution fusion | flops 206094336 | bytes 2195456 | tf_op jit(solution)/shard_map/dot_general | solution.py:71
  30.0 8.8 %all_gather.6 = bf16[512,128]{0,1:T(8,128)(2,1)} all-gather(bf16[128,128]{0,1:T(8,128)(2,1)S(1)} %concatenate.39), channel_id=1, replica_groups=mesh['sp_0'=16,'sp_1'=4,'tp'=8] {'sp_1'}, dimensions={0}, use_global_device_ids=true | all-gather | bytes 163840 | tf_op jit(solution)/shard_map/all_gather | solution.py:33
  38.8 0.0 all-gather.2.cloned.1.call-update
  38.9 0.1 mul.225
  39.0 0.1 broadcast_multiply_fusion.1
  39.1 0.1 fusion.37
  39.2 0.1 multiply_bitcast_fusion.1
  39.4 0.1 multiply_multiply_fusion
  39.5 64.0 %all-gather.2.cloned.1.call-done = bf16[8192,128]{0,1:T(8,128)(2,1)} async-done(((bf16[512,128]{0,1:T(8,128)(2,1)}), bf16[8192,128]{0,1:T(8,128)(2,1)}) %all-gather.2.cloned.1.call-update) | async-done | bytes 2097168 | tf_op jit(solution)/shard_map/all_gather | solution.py:33
  103.5 1.5 fusion.4
  105.1 1.5 fusion.5
  106.6 4.0 %subtract_convert_fusion = (bf16[8192,1,2,1,16]{0,4,3,2,1:T(8,128)(2,1)S(1)}, bf16[8192,1,2,1,16]{0,4,3,2,1:T(8,128)(2,1)S(1)}) fusion(f32[8192,1,2,2,16]{0,4,3,2,1:T(8,128)S(1)} %bitcast.33, f32[8192,1,1,1,16]{0,4,3,2,1:T(8,128)S(1)} %get-tuple-element.12, f32[8192,1,1,1,16]{0,4,3,2,1:T(8,128)S(1)} %get-tuple-element.11), kind=kLoop, calls=%fused_computation.24 | loop fusion | flops 2359296 | bytes 4194304 | tf_op jit(solution)/shard_map/convert.1
  110.6 0.1 pad_maximum_fusion.1
  110.7 8.1 %multiply_reduce_fusion = (f32[4,128]{1,0:T(4,128)S(1)}, f32[4,128,8192]{2,1,0:T(8,128)}) fusion(bf16[4,128,64]{1,2,0:T(8,128)(2,1)S(1)} %bitcast.39, bf16[8192,64,1]{0,1,2:T(8,128)(2,1)S(1)} %bitcast.34), kind=kOutput, calls=%fused_computation.1 | convolution fusion | flops 545259008 | bytes 17893376 | tf_op jit(solution)/shard_map/kgqd,nkd->kgqn/dot_general | solution.py:96
  118.8 8.8 %fusion = f32[4,128]{1,0:T(4,128)S(1)} fusion(f32[4,128,8192]{2,1,0:T(8,128)} %get-tuple-element.16, f32[4,128]{1,0:T(4,128)S(1)} %broadcast_maximum_fusion), kind=kLoop, calls=%fused_computation.2 | loop fusion | flops 12582400 | bytes 16781312 | tf_op jit(solution)/shard_map/reduce_sum | solution.py:100
  127.6 7.4 %fusion.21 = bf16[4,128,64]{1,2,0:T(8,128)(2,1)S(1)} fusion(f32[4,128,8192]{2,1,0:T(8,128)} %get-tuple-element.16, f32[4,128]{1,0:T(4,128)S(1)} %broadcast_maximum_fusion, bf16[8192,128]{0,1:T(8,128)(2,1)S(1)} %copy-done.1, f32[4,128]{1,0:T(4,128)S(1)} %fusion), kind=kOutput, calls=%fused_computation.19 | convolution fusion | flops 549519360 | bytes 17895424 | tf_op jit(solution)/shard_map/kgqn,nkd->kgqd/dot_general | solution.py:101
  135.0 0.3 convolution_convert_fusion
  135.3 23.1 %all_to_all.10 = bf16[8,16,2048]{2,1,0:T(8,128)(2,1)S(1)} all-to-all(bf16[8,16,2048]{2,1,0:T(8,128)(2,1)S(1)} %bitcast.35), channel_id=1, replica_groups=mesh['sp_0'=16,'sp_1'=4,'tp'=8] {'tp'}, dimensions={0} | all-to-all | bytes 1048576 | tf_op jit(solution)/shard_map/all_to_all | solution.py:44
  158.4 0.7 reduce_sum.42
  (20 shorter events, 0.2 us)
Async XLA Ops:
  6.5 128.5 %copy-start = (bf16[256,2048]{1,0:T(8,128)(2,1)S(1)}, bf16[256,2048]{1,0:T(8,128)(2,1)}, u32[]{:S(2)}) copy-start(bf16[256,2048]{1,0:T(8,128)(2,1)} %param.11) | copy-start | bytes 3145732
  8.3 19.6 %all-to-all-start = ((bf16[8,16,2048]{2,1,0:T(8,128)(2,1)}), bf16[8,16,2048]{2,1,0:T(8,128)(2,1)S(1)}, u32[]{:S(2)}, u32[]{:S(2)}) async-start(bf16[8,16,2048]{2,1,0:T(8,128)(2,1)} %broadcast_in_dim.4), calls=%async_computation | async-start | bytes 1048576 | tf_op jit(solution)/shard_map/all_to_all | solution.py:14
  18.5 85.0 %all-gather.2.cloned.1.call-start = ((), (), s32[]{:S(2)}) async-start(), calls=%async_computation.2 | async-start | bytes 2228224 | tf_op jit(solution)/shard_map/all_gather | solution.py:33
  19.8 19.1 %copy-start.2 = (f32[64]{0:T(128)S(1)}, f32[64]{0:T(128)}, u32[]{:S(2)}) copy-start(f32[64]{0:T(128)} %param.12) | copy-start | bytes 772
  27.9 77.1 %copy-start.3 = (f32[64]{0:T(128)S(1)}, f32[64]{0:T(128)}, u32[]{:S(2)}) copy-start(f32[64]{0:T(128)} %param.13) | copy-start | bytes 772
  118.8 8.8 %copy-start.1 = (bf16[8192,128]{0,1:T(8,128)(2,1)S(1)}, bf16[8192,128]{0,1:T(8,128)(2,1)}, u32[]{:S(2)}) copy-start(bf16[8192,128]{0,1:T(8,128)(2,1)} %all-gather.2.cloned.1.call-done) | copy-start | bytes 6291460
Sparse Core Ops, SparseCore 0:
  39.0 64.5 all-gather.1
where the time goes:
time: 166 us
  waiting for transfers between devices  70.9 us (43%)
  blocking collectives  31.9 us (19%)
  matrix products  17.9 us (11%)
  other arithmetic  17.1 us (10%)
  between operations  13.6 us (8%)
  starting transfers between devices  10.2 us (6%)
  local copies, waits for them, and re-layouts  4.36 us (3%)
    all_gather x1, waiting for transfers between devices, whole_of(): nearer = lax.all_gather(shard, axes[-1], axis=dim, tiled=True)  64 us
    all_to_all x1, blocking collectives, summed_on_arrival(): lax.all_to_all(blocks, axis, split_axis=0, concat_axis=0, tiled=True)  23.1 us
    all_to_all x1, starting transfers between devices, sent_to_all(): lax.all_to_all(jnp.broadcast_to(shard[None], (length, *shard.shape)), axi...  10.2 us
    all_gather x1, blocking collectives, whole_of(): nearer = lax.all_gather(shard, axes[-1], axis=dim, tiled=True)  8.8 us
    reduce_sum x1, other arithmetic, body(): total = jnp.sum(expo, axis=-1)  8.77 us
    dot_general x1, matrix products, body(): jnp.einsum('kgqd,nkd->kgqn', query_g, keys_n, preferred_element_type=jnp....  8.1 us
    dot_general x1, matrix products, body(): jnp.einsum('kgqn,nkd->kgqd', expo.astype(jnp.bfloat16), piece[:, key_cols...  7.43 us
    all_to_all x1, waiting for transfers between devices, sent_to_all(): lax.all_to_all(jnp.broadcast_to(shard[None], (length, *shard.shape)), axi...  6.87 us
  transfers between devices with their start and end apart: 2, of which 2 were waited for; matrix products, arithmetic and copies ran while one was open for 2% of the time, Pallas kernels for 0%

commit v1 on v0

v1 whole, which is shorter than its diff:
```python
import functools

import jax
import jax.numpy as jnp
from jax import lax
from jax.experimental import pallas as pl
from jax.experimental.pallas import tpu as pltpu
from jax.sharding import Mesh
from jax.sharding import PartitionSpec as P

F32, BF16 = jnp.float32, jnp.bfloat16
GRID_W = 64
SP = ("zq", "zp", "y")
TP = ("x", "c")
ALL = SP + TP
LOG2E = 1.4426950408889634
VMEM = pl.BlockSpec(memory_space=pltpu.VMEM)


def call(kernel, out, n_in, flops, byts, exps=0, limit=16, scratch=()):
    return pl.pallas_call(
        kernel,
        out_shape=out,
        in_specs=[VMEM] * n_in,
        out_specs=VMEM,
        scratch_shapes=list(scratch),
        compiler_params=pltpu.CompilerParams(vmem_limit_bytes=limit * 2**20),
        cost_estimate=pl.CostEstimate(flops=flops, bytes_accessed=byts, transcendentals=exps),
    )


def to_all(shard, axis):
    n = lax.axis_size(axis)
    return lax.all_to_all(
        jnp.broadcast_to(shard[None], (n, *shard.shape)), axis, 0, 0, tiled=True
    )


def turned(u, gain, tab):
    hd = u.shape[0]
    n = u * lax.rsqrt(jnp.sum(u * u, axis=0, keepdims=True) * (1.0 / hd) + 1e-6) * gain
    p = hd // 4
    out = []
    for half in range(2):
        a = n[half * 2 * p : half * 2 * p + p]
        b = n[half * 2 * p + p : half * 2 * p + 2 * p]
        cos, sin = tab[2 * half], tab[2 * half + 1]
        out += [a * cos - b * sin, a * sin + b * cos]
    return jnp.concatenate(out, axis=0)


def kv_kernel(copies, x_ref, wk_ref, wv_ref, gain_ref, tab_ref, out_ref):
    x = x_ref[...]
    k = jnp.dot(x, wk_ref[...], preferred_element_type=F32)
    v = jnp.dot(x, wv_ref[...], preferred_element_type=F32)
    kv = jnp.concatenate([k, v], axis=1).astype(BF16).astype(F32).T
    hd = k.shape[1]
    kt = turned(kv[:hd], gain_ref[...], tab_ref).astype(BF16)
    both = jnp.concatenate([kt, kv[hd:].astype(BF16)], axis=0)
    for i in range(copies):
        out_ref[i] = both


def q_kernel(copies, x_ref, w_ref, gain_ref, tab_ref, out_ref):
    q = jnp.dot(x_ref[...], w_ref[...], preferred_element_type=F32)
    qt = q.astype(BF16).astype(F32).T
    hd = gain_ref.shape[0]
    for h in range(qt.shape[0] // hd):
        rows = slice(h * hd, (h + 1) * hd)
        one = turned(qt[rows], gain_ref[...], tab_ref).astype(BF16)
        for i in range(copies):
            out_ref[i, rows] = one


def attend_kernel(hd, q_ref, kv_ref, out_ref, k_ref, v_ref):
    n_q, qc, rows = q_ref.shape
    n_k = kv_ref.shape[0]
    heads = qc // hd
    scale = hd**-0.5 * LOG2E
    for j in range(n_k):
        k_ref[j * rows : (j + 1) * rows, :] = kv_ref[j, :hd, :].astype(F32).T.astype(BF16)
        v_ref[16:, j * rows : (j + 1) * rows] = kv_ref[j, hd:, :]
    v_ref[:16, :] = jnp.ones((16, n_k * rows), BF16)

    def pair(i, _):
        tops, sums = [], []
        for h in range(heads):
            q = jnp.concatenate(
                [q_ref[2 * i + b, h * hd : (h + 1) * hd, :] for b in range(2)], axis=1
            )
            s = jnp.dot(k_ref[...], q, preferred_element_type=F32)
            top = (jnp.max(s, axis=0, keepdims=True) * scale).astype(BF16).astype(F32)
            p = jnp.exp2(s * scale - top).astype(BF16)
            o = jnp.dot(v_ref[...], p, preferred_element_type=F32)
            tops.append(top)
            sums.append(o[:1])
            for b in range(2):
                out_ref[2 * i + b, h * hd : (h + 1) * hd, :] = o[
                    16:, b * rows : (b + 1) * rows
                ].astype(BF16)
        total = jnp.concatenate(sums, axis=0)
        hi = total.astype(BF16).astype(F32)
        stats = jnp.concatenate(tops + [hi, total - hi, jnp.zeros_like(total)], axis=0).astype(BF16)
        for b in range(2):
            out_ref[2 * i + b, qc:, :] = stats[:, b * rows : (b + 1) * rows]
        return 0

    lax.fori_loop(0, n_q // 2, pair, 0)


def mix_kernel(hd, n_tp, got_ref, w_ref, out_ref, mixed_ref):
    parts, _, rows = got_ref.shape
    qc = w_ref.shape[0]
    heads = qc // hd
    st = [got_ref[i, qc:, :].astype(F32) for i in range(parts)]
    top = functools.reduce(jnp.maximum, [s[:heads] for s in st])
    factor = [jnp.exp2(s[:heads] - top) for s in st]
    total = functools.reduce(
        jnp.add,
        [f * (s[heads : 2 * heads] + s[2 * heads : 3 * heads]) for f, s in zip(factor, st)],
    )
    for h in range(heads):
        acc = 0.0
        for i in range(parts):
            acc += got_ref[i, h * hd : (h + 1) * hd, :].astype(F32) * factor[i][h : h + 1]
        mixed_ref[h * hd : (h + 1) * hd, :] = acc / total[h : h + 1]
    mixed = mixed_ref[...].T.astype(BF16)
    out = jnp.dot(mixed, w_ref[...], preferred_element_type=F32).astype(BF16)
    each = rows // n_tp
    for t in range(n_tp):
        out_ref[t % 2, t // 2] = out[t * each : (t + 1) * each]


def body(tokens_in, w_query, w_key, w_value, w_out, q_gain, k_gain):
    hd = q_gain.shape[0]
    qc = w_query.shape[1]
    mine, d = tokens_in.shape
    n_tp = lax.axis_size(TP)
    rows = mine * n_tp
    n_k = lax.axis_size("zq")
    n_q = lax.axis_size(("zp", "y"))
    heads = qc // hd

    tokens = to_all(tokens_in, TP).reshape(rows, d)
    position = lax.axis_index(SP) * rows + jnp.arange(rows, dtype=jnp.int32)
    pairs = hd // 4
    freq = 10000.0 ** (-jnp.arange(pairs, dtype=F32) / pairs)
    grid = jnp.stack([position // GRID_W, position % GRID_W]).astype(F32)
    angle = grid[:, None, :] * freq[None, :, None]
    tab = jnp.stack([jnp.cos(angle), jnp.sin(angle)], axis=1).reshape(4, pairs, rows)
    gains = [jnp.broadcast_to(g[:, None], (hd, rows)) for g in (q_gain, k_gain)]

    kv = call(
        functools.partial(kv_kernel, n_k),
        jax.ShapeDtypeStruct((n_k, 2 * hd, rows), BF16),
        5,
        2 * rows * d * 2 * hd,
        2 * d * (rows + 2 * hd),
    )(tokens, w_key, w_value, gains[1], tab)
    kv = lax.all_to_all(kv, "zq", 0, 0, tiled=True)

    query = call(
        functools.partial(q_kernel, n_q),
        jax.ShapeDtypeStruct((n_q, qc, rows), BF16),
        4,
        2 * rows * d * qc,
        2 * d * (rows + qc),
    )(tokens, w_query, gains[0], tab)
    query = lax.all_to_all(query, ("zp", "y"), 0, 0, tiled=True)

    part = call(
        functools.partial(attend_kernel, hd),
        jax.ShapeDtypeStruct((n_q, qc + 16, rows), BF16),
        2,
        4 * heads * n_q * rows * n_k * rows * hd,
        4 * n_q * qc * rows,
        exps=heads * n_q * rows * n_k * rows,
        limit=32,
        scratch=(
            pltpu.VMEM((n_k * rows, hd), BF16),
            pltpu.VMEM((hd + 16, n_k * rows), BF16),
        ),
    )(query, kv)
    got = lax.all_to_all(part, ("zp", "y"), 0, 0, tiled=True)

    partial = call(
        functools.partial(mix_kernel, hd, n_tp),
        jax.ShapeDtypeStruct((2, n_tp // 2, mine, d), BF16),
        2,
        2 * rows * qc * d,
        2 * d * (rows + qc),
        scratch=(pltpu.VMEM((qc, rows), F32),),
    )(got, w_out)
    near = lax.all_to_all(partial, "c", 0, 0, tiled=True)
    near = near.astype(F32).sum(axis=0).astype(BF16)
    far = lax.all_to_all(near, "x", 0, 0, tiled=True)
    return far.astype(F32).sum(axis=0).astype(BF16)


def solution(mesh):
    finer = Mesh(mesh.devices.reshape(8, 2, 4, mesh.shape["tp"] // 2, 2), ALL)
    return jax.shard_map(
        body,
        mesh=finer,
        in_specs=(
            P(ALL, None),
            P(None, TP),
            P(None, TP),
            P(None, TP),
            P(TP, None),
            P(),
            P(),
        ),
        out_specs=P(ALL, None),
        check_vma=False,
    )
```

time: 166 us -> 107 us (0.64)
  waiting for transfers between devices: 70.9 us -> 23.9 us
  matrix products: 17.9 us -> 0 us
  other arithmetic: 17.1 us -> 0.97 us
  Pallas kernels: 0 us -> 13.8 us
  between operations: 13.6 us -> 0.1 us
  blocking collectives: 31.9 us -> 43 us
  starting transfers between devices: 10.2 us -> 20.8 us
    all_gather x1 -> x0, waiting for transfers between devices: 64 us -> none  [whole_of(): nearer = lax.all_gather(shard, axes[-1], axis=dim, tiled=True)]
    all_to_all x1 -> x4, blocking collectives: 23.1 us -> 43 us  [the longest x1 12.4 us: body(): near = lax.all_to_all(partial, 'c', 0, 0, tiled=True)]
    dot_general x4 -> x0, matrix products: 17.9 us -> none  [the longest x1 8.1 us: body(): jnp.einsum('kgqd,nkd->kgqn', query_g, keys_n, preferred_element_type=jnp....]
    all_to_all x1 -> x2, waiting for transfers between devices: 6.87 us -> 23.9 us  [the longest x1 16 us: body(): kv = lax.all_to_all(kv, 'zq', 0, 0, tiled=True)]
    pallas_call x0 -> x4, Pallas kernels: none -> 13.8 us  [the longest x1 11.6 us: body(): call(functools.partial(attend_kernel, hd), jax.ShapeDtypeStruct((n_q, qc...]
    all_to_all x1 -> x2, starting transfers between devices: 10.2 us -> 20.8 us  [the longest x1 10.5 us: body(): kv = lax.all_to_all(kv, 'zq', 0, 0, tiled=True)]
    reduce_sum x4 -> x2, other arithmetic: 11 us -> 0.8 us  [the longest x1 0.67 us: body(): return far.astype(F32).sum(axis=0).astype(BF16)]
    all_gather x1 -> x0, blocking collectives: 8.8 us -> none  [whole_of(): nearer = lax.all_gather(shard, axes[-1], axis=dim, tiled=True)]
  transfers between devices with their start and end apart: 2 -> 2, of which waited for: 2 -> 2; matrix products, arithmetic and copies ran while one was open for 2% -> 1% of each run, Pallas kernels for 0% -> 0%
where the time goes in v1:
time: 107 us; the launch traced here: 106 us
  blocking collectives  43 us (40%)
  waiting for transfers between devices  23.9 us (22%)
  starting transfers between devices  20.8 us (19%)
  Pallas kernels  13.8 us (13%)
  local copies, waits for them, and re-layouts  3.71 us (3%)
    all_to_all x1, waiting for transfers between devices, body(): kv = lax.all_to_all(kv, 'zq', 0, 0, tiled=True)  16 us
    all_to_all x1, blocking collectives, body(): near = lax.all_to_all(partial, 'c', 0, 0, tiled=True)  12.4 us
    pallas_call x1, Pallas kernels, body(): call(functools.partial(attend_kernel, hd), jax.ShapeDtypeStruct((n_q, qc...  11.6 us
    all_to_all x1, blocking collectives, body(): query = lax.all_to_all(query, ('zp', 'y'), 0, 0, tiled=True)  11.5 us
    all_to_all x1, starting transfers between devices, body(): kv = lax.all_to_all(kv, 'zq', 0, 0, tiled=True)  10.5 us
    all_to_all x1, blocking collectives, body(): got = lax.all_to_all(part, ('zp', 'y'), 0, 0, tiled=True)  10.4 us
    all_to_all x1, starting transfers between devices, to_all(): lax.all_to_all(jnp.broadcast_to(shard[None], (n, *shard.shape)), axis, 0,...  10.4 us
    all_to_all x1, blocking collectives, body(): far = lax.all_to_all(near, 'x', 0, 0, tiled=True)  8.78 us
  transfers between devices with their start and end apart: 2, of which 2 were waited for; matrix products, arithmetic and copies ran while one was open for 1% of the time, Pallas kernels for 0%

profile of v1, /device:TPU:1, one launch (start us, length us, event | category | flops | bytes accessed | tf_op | source)
XLA Modules:
  0.0 106.4 jit_solution(13986888221465167647)
XLA Ops:
  0.0 1.7 %broadcast_in_dim.6 = bf16[8,16,2048]{2,1,0:T(8,128)(2,1)} broadcast(bf16[16,2048]{1,0:T(8,128)(2,1)} %param.7), dimensions={1,2} | broadcast | bytes 589824 | tf_op jit(solution)/shard_map/broadcast_in_dim | solution.py:35
  1.7 10.4 %all-to-all-start = ((bf16[8,16,2048]{2,1,0:T(8,128)(2,1)}), bf16[8,16,2048]{2,1,0:T(8,128)(2,1)S(1)}, u32[]{:S(2)}, u32[]{:S(2)}) async-start(bf16[8,16,2048]{2,1,0:T(8,128)(2,1)} %broadcast_in_dim.6), calls=%async_computation | async-start | bytes 1048576 | tf_op jit(solution)/shard_map/all_to_all | solution.py:34
  12.1 0.0 copy-start.3
  12.1 0.3 copy.10.wk_ref
  12.4 0.7 copy-done.3
  13.0 0.3 copy.11.wv_ref
  13.3 0.1 multiply_cosine_fusion
  13.5 7.9 %all-to-all-done = bf16[8,16,2048]{2,1,0:T(8,128)(2,1)S(1)} async-done(((bf16[8,16,2048]{2,1,0:T(8,128)(2,1)}), bf16[8,16,2048]{2,1,0:T(8,128)(2,1)S(1)}, u32[]{:S(2)}, u32[]{:S(2)}) %all-to-all-start) | async-done | bytes 524320 | tf_op jit(solution)/shard_map/all_to_all | solution.py:34
  21.4 0.7 copy-done.4
  22.1 0.1 broadcast_in_dim.8.gain_ref
  22.2 1.3 %shard_map.74 = bf16[8,128,128]{2,1,0:T(8,128)(2,1)} custom-call(bf16[128,2048]{1,0:T(8,128)(2,1)S(1)} %bitcast.2, bf16[2048,64]{1,0:T(8,128)(2,1)S(1)} %copy.10.wk_ref, bf16[2048,64]{1,0:T(8,128)(2,1)S(1)} %copy.11.wv_ref, f32[64,128]{1,0:T(8,128)S(1)} %broadcast_in_dim.8.gain_ref, f32[4,16,128]{2,1,0:T(8,128)S(1)} %bitcast.4), custom_call_target="tpu_custom_call" | custom-call | flops 67108864 | bytes 1048576 | tf_op jit(solution)/shard_map/pallas_call | solution.py:153
  23.5 10.5 %all-to-all-start.2 = ((bf16[8,128,128]{2,1,0:T(8,128)(2,1)}), bf16[8,128,128]{2,1,0:T(8,128)(2,1)S(1)}, u32[]{:S(2)}, u32[]{:S(2)}) async-start(bf16[8,128,128]{2,1,0:T(8,128)(2,1)} %shard_map.74), calls=%async_computation.2 | async-start | bytes 524288 | tf_op jit(solution)/shard_map/all_to_all | solution.py:160
  33.9 0.1 broadcast_in_dim.7.gain_ref
  34.0 0.4 shard_map.73
  34.4 16.0 %all-to-all-done.2.kv_ref = bf16[8,128,128]{2,1,0:T(8,128)(2,1)S(1)} async-done(((bf16[8,128,128]{2,1,0:T(8,128)(2,1)}), bf16[8,128,128]{2,1,0:T(8,128)(2,1)S(1)}, u32[]{:S(2)}, u32[]{:S(2)}) %all-to-all-start.2) | async-done | bytes 262176 | tf_op jit(solution)/shard_map/all_to_all | solution.py:160
  50.4 11.5 %all_to_all.30.q_ref = bf16[8,256,128]{2,1,0:T(8,128)(2,1)S(1)} all-to-all(bf16[8,256,128]{2,1,0:T(8,128)(2,1)S(1)} %shard_map.73), channel_id=1, replica_groups=mesh['zq'=8,'zp'=2,'y'=4,'x'=4,'c'=2] {'zp','y'}, dimensions={0} | all-to-all | bytes 1048576 | tf_op jit(solution)/shard_map/all_to_all | solution.py:169
  61.9 11.6 %shard_map.75 = bf16[8,272,128]{2,1,0:T(8,128)(2,1)S(1)} custom-call(bf16[8,256,128]{2,1,0:T(8,128)(2,1)S(1)} %all_to_all.30.q_ref, bf16[8,128,128]{2,1,0:T(8,128)(2,1)S(1)} %all-to-all-done.2.kv_ref), custom_call_target="tpu_custom_call" | custom-call | flops 1073741824 | bytes 1048576 | tf_op jit(solution)/shard_map/pallas_call | solution.py:171
  73.5 0.0 copy-start.1
  73.5 10.4 %all_to_all.31.got_ref = bf16[8,272,128]{2,1,0:T(8,128)(2,1)S(1)} all-to-all(bf16[8,272,128]{2,1,0:T(8,128)(2,1)S(1)} %shard_map.75), channel_id=1, replica_groups=mesh['zq'=8,'zp'=2,'y'=4,'x'=4,'c'=2] {'zp','y'}, dimensions={0} | all-to-all | bytes 1114112 | tf_op jit(solution)/shard_map/all_to_all | solution.py:184
  84.0 0.4 shard_map.76
  84.4 12.4 %all_to_all.32 = bf16[2,4,16,2048]{3,2,1,0:T(8,128)(2,1)S(1)} all-to-all(bf16[2,4,16,2048]{3,2,1,0:T(8,128)(2,1)S(1)} %shard_map.76), channel_id=1, replica_groups=mesh['zq'=8,'zp'=2,'y'=4,'x'=4,'c'=2] {'c'}, dimensions={0} | all-to-all | bytes 1048576 | tf_op jit(solution)/shard_map/all_to_all | solution.py:194
  96.8 0.1 reduce_sum.24
  96.9 8.8 %all_to_all.33 = bf16[4,16,2048]{2,1,0:T(8,128)(2,1)S(1)} all-to-all(bf16[4,16,2048]{2,1,0:T(8,128)(2,1)S(1)} %reduce_sum.24), channel_id=1, replica_groups=mesh['zq'=8,'zp'=2,'y'=4,'x'=4,'c'=2] {'x'}, dimensions={0} | all-to-all | bytes 524288 | tf_op jit(solution)/shard_map/all_to_all | solution.py:196
  105.7 0.7 reduce_sum.25
  (12 shorter events, 0.1 us)
Async XLA Ops:
  1.7 10.4 %copy-start.2 = (bf16[2048,64]{0,1:T(8,128)(2,1)S(1)}, bf16[2048,64]{0,1:T(8,128)(2,1)}, u32[]{:S(2)}) copy-start(bf16[2048,64]{0,1:T(8,128)(2,1)} %param.9) | copy-start | bytes 786436
  1.7 19.7 %all-to-all-start = ((bf16[8,16,2048]{2,1,0:T(8,128)(2,1)}), bf16[8,16,2048]{2,1,0:T(8,128)(2,1)S(1)}, u32[]{:S(2)}, u32[]{:S(2)}) async-start(bf16[8,16,2048]{2,1,0:T(8,128)(2,1)} %broadcast_in_dim.6), calls=%async_computation | async-start | bytes 1048576 | tf_op jit(solution)/shard_map/all_to_all | solution.py:34
  12.1 1.0 copy-start.3
  21.4 0.7 copy-start.4
  22.2 11.8 %copy-start = (bf16[2048,256]{1,0:T(8,128)(2,1)S(1)}, bf16[2048,256]{1,0:T(8,128)(2,1)}, u32[]{:S(2)}) copy-start(bf16[2048,256]{1,0:T(8,128)(2,1)} %w_ref.2) | copy-start | bytes 3145732
  23.4 10.5 %copy-start.5 = (f32[64]{0:T(128)S(1)}, f32[64]{0:T(128)}, u32[]{:S(2)}) copy-start(f32[64]{0:T(128)} %param.12) | copy-start | bytes 772
  23.5 27.0 %all-to-all-start.2 = ((bf16[8,128,128]{2,1,0:T(8,128)(2,1)}), bf16[8,128,128]{2,1,0:T(8,128)(2,1)S(1)}, u32[]{:S(2)}, u32[]{:S(2)}) async-start(bf16[8,128,128]{2,1,0:T(8,128)(2,1)} %shard_map.74), calls=%async_computation.2 | async-start | bytes 524288 | tf_op jit(solution)/shard_map/all_to_all | solution.py:160
  73.5 10.4 %copy-start.1 = (bf16[256,2048]{1,0:T(8,128)(2,1)S(1)}, bf16[256,2048]{1,0:T(8,128)(2,1)}, u32[]{:S(2)}) copy-start(bf16[256,2048]{1,0:T(8,128)(2,1)} %w_ref.3) | copy-start | bytes 3145732

commit v2 on v1

--- a/solution.py
+++ b/solution.py
@@ -7,6 +7,7 @@
 from jax.experimental.pallas import tpu as pltpu
 from jax.sharding import Mesh
 from jax.sharding import PartitionSpec as P
+
 
 F32, BF16 = jnp.float32, jnp.bfloat16
 GRID_W = 64
@@ -36,46 +37,64 @@
     )
 
 
-def turned(u, gain, tab):
+def table_kernel(qg_ref, kg_ref, tab_ref, out_ref):
+    p = tab_ref.shape[1]
+    for i, ref in enumerate((qg_ref, kg_ref)):
+        gain = jnp.broadcast_to(ref[...], (tab_ref.shape[2], ref.shape[1])).T
+        for half in range(2):
+            cos, sin = tab_ref[2 * half], tab_ref[2 * half + 1]
+            a, b = 2 * half * p, (2 * half + 1) * p
+            ga, gb = gain[a : a + p], gain[b : b + p]
+            out_ref[i, 0, a : a + p] = ga * cos
+            out_ref[i, 0, b : b + p] = gb * cos
+            out_ref[i, 1, a : a + p] = -gb * sin
+            out_ref[i, 1, b : b + p] = ga * sin
+
+
+def turned(u, cos, sin):
     hd = u.shape[0]
-    n = u * lax.rsqrt(jnp.sum(u * u, axis=0, keepdims=True) * (1.0 / hd) + 1e-6) * gain
     p = hd // 4
-    out = []
-    for half in range(2):
-        a = n[half * 2 * p : half * 2 * p + p]
-        b = n[half * 2 * p + p : half * 2 * p + 2 * p]
-        cos, sin = tab[2 * half], tab[2 * half + 1]
-        out += [a * cos - b * sin, a * sin + b * cos]
-    return jnp.concatenate(out, axis=0)
-
-
-def kv_kernel(copies, x_ref, wk_ref, wv_ref, gain_ref, tab_ref, out_ref):
+    swapped = jnp.concatenate([u[p : 2 * p], u[:p], u[3 * p :], u[2 * p : 3 * p]], axis=0)
+    inv = lax.rsqrt(jnp.sum(u * u, axis=0, keepdims=True) * (1.0 / hd) + 1e-6)
+    return (u * inv) * cos + (swapped * inv) * sin
+
+
+NT = (((1,), (1,)), ((), ()))
+
+
+def kv_kernel(copies, x_ref, wk_ref, wv_ref, tab_ref, out_ref):
     x = x_ref[...]
-    k = jnp.dot(x, wk_ref[...], preferred_element_type=F32)
-    v = jnp.dot(x, wv_ref[...], preferred_element_type=F32)
-    kv = jnp.concatenate([k, v], axis=1).astype(BF16).astype(F32).T
-    hd = k.shape[1]
-    kt = turned(kv[:hd], gain_ref[...], tab_ref).astype(BF16)
-    both = jnp.concatenate([kt, kv[hd:].astype(BF16)], axis=0)
+    k = lax.dot_general(wk_ref[...], x, NT, preferred_element_type=F32)
+    v = lax.dot_general(wv_ref[...], x, NT, preferred_element_type=F32)
+    kt = turned(k.astype(BF16).astype(F32), tab_ref[1, 0], tab_ref[1, 1]).astype(BF16)
+    both = jnp.concatenate([kt, v.astype(BF16)], axis=0)
     for i in range(copies):
         out_ref[i] = both
 
 
-def q_kernel(copies, x_ref, w_ref, gain_ref, tab_ref, out_ref):
+def q_kernel(x_ref, w_ref, tab_ref, out_ref):
     q = jnp.dot(x_ref[...], w_ref[...], preferred_element_type=F32)
     qt = q.astype(BF16).astype(F32).T
-    hd = gain_ref.shape[0]
+    hd = tab_ref.shape[2]
     for h in range(qt.shape[0] // hd):
         rows = slice(h * hd, (h + 1) * hd)
-        one = turned(qt[rows], gain_ref[...], tab_ref).astype(BF16)
-        for i in range(copies):
-            out_ref[i, rows] = one
+        out_ref[0, rows] = turned(qt[rows], tab_ref[0, 0], tab_ref[0, 1]).astype(BF16)
+
+
+def pair_kernel(hd, q_ref, out_ref):
+    n_q, qc, rows = q_ref.shape
+    for i in range(n_q):
+        for h in range(qc // hd):
+            out_ref[i // 2, h, :, (i % 2) * rows : (i % 2 + 1) * rows] = q_ref[
+                i, h * hd : (h + 1) * hd, :
+            ]
 
 
 def attend_kernel(hd, q_ref, kv_ref, out_ref, k_ref, v_ref):
-    n_q, qc, rows = q_ref.shape
+    n_pair, heads, _, rows = q_ref.shape
+    rows //= 2
     n_k = kv_ref.shape[0]
-    heads = qc // hd
+    qc = heads * hd
     scale = hd**-0.5 * LOG2E
     for j in range(n_k):
         k_ref[j * rows : (j + 1) * rows, :] = kv_ref[j, :hd, :].astype(F32).T.astype(BF16)
@@ -85,10 +104,7 @@
     def pair(i, _):
         tops, sums = [], []
         for h in range(heads):
-            q = jnp.concatenate(
-                [q_ref[2 * i + b, h * hd : (h + 1) * hd, :] for b in range(2)], axis=1
-            )
-            s = jnp.dot(k_ref[...], q, preferred_element_type=F32)
+            s = jnp.dot(k_ref[...], q_ref[i, h], preferred_element_type=F32)
             top = (jnp.max(s, axis=0, keepdims=True) * scale).astype(BF16).astype(F32)
             p = jnp.exp2(s * scale - top).astype(BF16)
             o = jnp.dot(v_ref[...], p, preferred_element_type=F32)
@@ -105,7 +121,7 @@
             out_ref[2 * i + b, qc:, :] = stats[:, b * rows : (b + 1) * rows]
         return 0
 
-    lax.fori_loop(0, n_q // 2, pair, 0)
+    lax.fori_loop(0, n_pair, pair, 0)
 
 
 def mix_kernel(hd, n_tp, got_ref, w_ref, out_ref, mixed_ref):
@@ -128,7 +144,7 @@
     out = jnp.dot(mixed, w_ref[...], preferred_element_type=F32).astype(BF16)
     each = rows // n_tp
     for t in range(n_tp):
-        out_ref[t % 2, t // 2] = out[t * each : (t + 1) * each]
+        out_ref[t] = out[t * each : (t + 1) * each]
 
 
 def body(tokens_in, w_query, w_key, w_value, w_out, q_gain, k_gain):
@@ -141,32 +157,46 @@
     n_q = lax.axis_size(("zp", "y"))
     heads = qc // hd
 
-    tokens = to_all(tokens_in, TP).reshape(rows, d)
     position = lax.axis_index(SP) * rows + jnp.arange(rows, dtype=jnp.int32)
     pairs = hd // 4
     freq = 10000.0 ** (-jnp.arange(pairs, dtype=F32) / pairs)
     grid = jnp.stack([position // GRID_W, position % GRID_W]).astype(F32)
     angle = grid[:, None, :] * freq[None, :, None]
     tab = jnp.stack([jnp.cos(angle), jnp.sin(angle)], axis=1).reshape(4, pairs, rows)
-    gains = [jnp.broadcast_to(g[:, None], (hd, rows)) for g in (q_gain, k_gain)]
+    tab = call(
+        table_kernel,
+        jax.ShapeDtypeStruct((2, 2, hd, rows), F32),
+        3,
+        8 * hd * rows,
+        32 * hd * rows,
+    )(q_gain[None], k_gain[None], tab)
+    tokens_in, tab = lax.optimization_barrier((tokens_in, tab))
+    tokens = to_all(tokens_in, TP).reshape(rows, d)
 
     kv = call(
         functools.partial(kv_kernel, n_k),
         jax.ShapeDtypeStruct((n_k, 2 * hd, rows), BF16),
-        5,
+        4,
         2 * rows * d * 2 * hd,
         2 * d * (rows + 2 * hd),
-    )(tokens, w_key, w_value, gains[1], tab)
+    )(tokens, w_key.T, w_value.T, tab)
     kv = lax.all_to_all(kv, "zq", 0, 0, tiled=True)
 
     query = call(
-        functools.partial(q_kernel, n_q),
-        jax.ShapeDtypeStruct((n_q, qc, rows), BF16),
-        4,
+        q_kernel,
+        jax.ShapeDtypeStruct((1, qc, rows), BF16),
+        3,
         2 * rows * d * qc,
         2 * d * (rows + qc),
-    )(tokens, w_query, gains[0], tab)
-    query = lax.all_to_all(query, ("zp", "y"), 0, 0, tiled=True)
+    )(tokens, w_query, tab)
+    query = lax.all_gather(query, ("zp", "y"), axis=0, tiled=True)
+    query = call(
+        functools.partial(pair_kernel, hd),
+        jax.ShapeDtypeStruct((n_q // 2, heads, hd, 2 * rows), BF16),
+        1,
+        n_q * qc * rows,
+        4 * n_q * qc * rows,
+    )(query)
 
     part = call(
         functools.partial(attend_kernel, hd),
@@ -185,20 +215,19 @@
 
     partial = call(
         functools.partial(mix_kernel, hd, n_tp),
-        jax.ShapeDtypeStruct((2, n_tp // 2, mine, d), BF16),
+        jax.ShapeDtypeStruct((n_tp, mine, d), BF16),
         2,
         2 * rows * qc * d,
         2 * d * (rows + qc),
         scratch=(pltpu.VMEM((qc, rows), F32),),
     )(got, w_out)
-    near = lax.all_to_all(partial, "c", 0, 0, tiled=True)
-    near = near.astype(F32).sum(axis=0).astype(BF16)
-    far = lax.all_to_all(near, "x", 0, 0, tiled=True)
-    return far.astype(F32).sum(axis=0).astype(BF16)
+    got = lax.all_to_all(partial, TP, 0, 0, tiled=True)
+    return got.astype(F32).sum(axis=0).astype(BF16)
 
 
 def solution(mesh):
     finer = Mesh(mesh.devices.reshape(8, 2, 4, mesh.shape["tp"] // 2, 2), ALL)
+
     return jax.shard_map(
         body,
         mesh=finer,

time: 107 us -> 108 us (level)
  blocking collectives: 43 us -> 80.2 us
  waiting for transfers between devices: 23.9 us -> 0.01 us
  starting transfers between devices: 20.8 us -> 11.2 us
  local copies, waits for them, and re-layouts: 3.71 us -> 1.47 us
    all_gather x0 -> x1, blocking collectives: none -> 26.4 us  [body(): query = lax.all_gather(query, ('zp', 'y'), axis=0, tiled=True)]
    all_to_all x1, waiting for transfers between devices: 16 us -> 0.01 us  [body(): kv = lax.all_to_all(kv, 'zq', 0, 0, tiled=True)]
    all_to_all x1 -> x0, starting transfers between devices: 10.4 us -> none  [to_all(): lax.all_to_all(jnp.broadcast_to(shard[None], (n, *shard.shape)), axis, 0,...]
    all_to_all x1 -> x0, waiting for transfers between devices: 7.94 us -> none  [to_all(): lax.all_to_all(jnp.broadcast_to(shard[None], (n, *shard.shape)), axis, 0,...]
    all_to_all x3 -> x2, blocking collectives: 32.6 us -> 40.1 us  [the longest x1 21.4 us: body(): got = lax.all_to_all(partial, TP, 0, 0, tiled=True)]
    all_to_all x1, blocking collectives: 10.4 us -> 13.7 us  [body(): got = lax.all_to_all(part, ('zp', 'y'), 0, 0, tiled=True)]
    broadcast_in_dim x1, local copies, waits for them, and re-layouts: 1.68 us -> 0.04 us  [to_all(): jnp.broadcast_to(shard[None], (n, *shard.shape))]
  transfers between devices with their start and end apart: 2 -> 1, of which waited for: 2 -> 0; matrix products, arithmetic and copies ran while one was open for 1% -> 0% of each run, Pallas kernels for 0% -> 0%
where the time goes in v2:
time: 108 us
  blocking collectives  80.2 us (74%)
  Pallas kernels  13.8 us (13%)
  starting transfers between devices  11.2 us (10%)
  local copies, waits for them, and re-layouts  1.47 us (1%)
    all_gather x1, blocking collectives, body(): query = lax.all_gather(query, ('zp', 'y'), axis=0, tiled=True)  26.4 us
    all_to_all x1, blocking collectives, body(): got = lax.all_to_all(partial, TP, 0, 0, tiled=True)  21.4 us
    all_to_all x1, blocking collectives, to_all(): lax.all_to_all(jnp.broadcast_to(shard[None], (n, *shard.shape)), axis, 0,...  18.7 us
    all_to_all x1, blocking collectives, body(): got = lax.all_to_all(part, ('zp', 'y'), 0, 0, tiled=True)  13.7 us
    pallas_call x1, Pallas kernels, body(): call(functools.partial(attend_kernel, hd), jax.ShapeDtypeStruct((n_q, qc...  11.6 us
    all_to_all x1, starting transfers between devices, body(): kv = lax.all_to_all(kv, 'zq', 0, 0, tiled=True)  11.2 us
  transfers between devices with their start and end apart: 1, of which 0 were waited for; matrix products, arithmetic and copies ran while one was open for 0% of the time, Pallas kernels for 0%

profile of v2, /device:TPU:1, one launch (start us, length us, event | category | flops | bytes accessed | tf_op | source)
XLA Modules:
  0.0 107.6 jit_solution(6834565286346668543)
XLA Ops:
  0.1 0.1 multiply_cosine_fusion
  0.2 0.0 copy-start.4
  0.2 0.0 copy-start.5
  0.2 0.6 copy-done.4
  0.9 0.0 copy-done.5
  0.9 0.1 shard_map.73.tab_ref
  1.0 0.7 copy-done.6
  1.8 0.0 copy-start.2
  1.8 0.0 copy-start.3
  1.8 18.7 %all_to_all.20 = bf16[8,16,2048]{2,1,0:T(8,128)(2,1)S(1)} all-to-all(bf16[8,16,2048]{2,1,0:T(8,128)(2,1)S(1)} %broadcast_in_dim.16), channel_id=1, replica_groups=mesh['zq'=8,'zp'=2,'y'=4,'x'=4,'c'=2] {'x','c'}, dimensions={0} | all-to-all | bytes 1048576 | tf_op jit(solution)/shard_map/all_to_all | solution.py:35
  20.5 0.0 copy-done.2
  20.5 1.2 %shard_map.76 = bf16[8,128,128]{2,1,0:T(8,128)(2,1)} custom-call(bf16[128,2048]{1,0:T(8,128)(2,1)S(1)} %bitcast.6, bf16[64,2048]{1,0:T(8,128)(2,1)S(1)} %bitcast.8, bf16[64,2048]{1,0:T(8,128)(2,1)S(1)} %bitcast.9, f32[2,2,64,128]{3,2,1,0:T(8,128)S(1)} %shard_map.73.tab_ref), custom_call_target="tpu_custom_call" | custom-call | flops 67108864 | bytes 1048576 | tf_op jit(solution)/shard_map/pallas_call | solution.py:176
  21.7 11.2 %all-to-all-start.1 = ((bf16[8,128,128]{2,1,0:T(8,128)(2,1)}), bf16[8,128,128]{2,1,0:T(8,128)(2,1)S(1)}, u32[]{:S(2)}, u32[]{:S(2)}) async-start(bf16[8,128,128]{2,1,0:T(8,128)(2,1)} %shard_map.76), calls=%async_computation.1 | async-start | bytes 524288 | tf_op jit(solution)/shard_map/all_to_all | solution.py:183
  32.8 0.0 copy-done
  32.9 0.4 shard_map.74
  33.3 26.4 %all_gather.3.q_ref = bf16[8,256,128]{2,1,0:T(8,128)(2,1)S(1)} all-gather(bf16[1,256,128]{2,1,0:T(8,128)(2,1)S(1)} %shard_map.74), channel_id=1, replica_groups=mesh['zq'=8,'zp'=2,'y'=4,'x'=4,'c'=2] {'zp','y'}, dimensions={0}, use_global_device_ids=true | all-gather | bytes 589824 | tf_op jit(solution)/shard_map/all_gather | solution.py:192
  59.7 0.1 shard_map.75.q_ref
  59.8 0.0 all-to-all-done.1.kv_ref
  59.8 11.6 %shard_map.77 = bf16[8,272,128]{2,1,0:T(8,128)(2,1)S(1)} custom-call(bf16[4,4,64,256]{3,2,1,0:T(8,128)(2,1)S(1)} %shard_map.75.q_ref, bf16[8,128,128]{2,1,0:T(8,128)(2,1)S(1)} %all-to-all-done.1.kv_ref), custom_call_target="tpu_custom_call" | custom-call | flops 1073741824 | bytes 1048576 | tf_op jit(solution)/shard_map/pallas_call | solution.py:201
  71.4 0.0 copy-start.1
  71.4 13.7 %all_to_all.21.got_ref = bf16[8,272,128]{2,1,0:T(8,128)(2,1)S(1)} all-to-all(bf16[8,272,128]{2,1,0:T(8,128)(2,1)S(1)} %shard_map.77), channel_id=1, replica_groups=mesh['zq'=8,'zp'=2,'y'=4,'x'=4,'c'=2] {'zp','y'}, dimensions={0} | all-to-all | bytes 1114112 | tf_op jit(solution)/shard_map/all_to_all | solution.py:214
  85.1 0.4 shard_map.78
  85.6 21.4 %all_to_all.22 = bf16[8,16,2048]{2,1,0:T(8,128)(2,1)S(1)} all-to-all(bf16[8,16,2048]{2,1,0:T(8,128)(2,1)S(1)} %shard_map.78), channel_id=1, replica_groups=mesh['zq'=8,'zp'=2,'y'=4,'x'=4,'c'=2] {'x','c'}, dimensions={0} | all-to-all | bytes 1048576 | tf_op jit(solution)/shard_map/all_to_all | solution.py:224
  106.9 0.7 reduce_sum.12
  (9 shorter events, 0.1 us)
Async XLA Ops:
  0.2 0.7 copy-start.4
  0.2 0.7 copy-start.5
  0.9 0.8 copy-start.6
  1.8 18.7 %copy-start.2 = (bf16[2048,64]{0,1:T(8,128)(2,1)S(1)}, bf16[2048,64]{0,1:T(8,128)(2,1)}, u32[]{:S(2)}) copy-start(bf16[2048,64]{0,1:T(8,128)(2,1)} %param.9) | copy-start | bytes 786436
  1.8 18.7 %copy-start.3 = (bf16[2048,64]{0,1:T(8,128)(2,1)S(1)}, bf16[2048,64]{0,1:T(8,128)(2,1)}, u32[]{:S(2)}) copy-start(bf16[2048,64]{0,1:T(8,128)(2,1)} %param.10) | copy-start | bytes 786436
  20.5 12.4 %copy-start = (bf16[2048,256]{1,0:T(8,128)(2,1)S(1)}, bf16[2048,256]{1,0:T(8,128)(2,1)}, u32[]{:S(2)}) copy-start(bf16[2048,256]{1,0:T(8,128)(2,1)} %w_ref.2) | copy-start | bytes 3145732
  21.7 38.1 %all-to-all-start.1 = ((bf16[8,128,128]{2,1,0:T(8,128)(2,1)}), bf16[8,128,128]{2,1,0:T(8,128)(2,1)S(1)}, u32[]{:S(2)}, u32[]{:S(2)}) async-start(bf16[8,128,128]{2,1,0:T(8,128)(2,1)} %shard_map.76), calls=%async_computation.1 | async-start | bytes 524288 | tf_op jit(solution)/shard_map/all_to_all | solution.py:183
  71.4 13.7 %copy-start.1 = (bf16[256,2048]{1,0:T(8,128)(2,1)S(1)}, bf16[256,2048]{1,0:T(8,128)(2,1)}, u32[]{:S(2)}) copy-start(bf16[256,2048]{1,0:T(8,128)(2,1)} %w_ref.3) | copy-start | bytes 3145732

commit v3 on v2

--- a/solution.py
+++ b/solution.py
@@ -78,16 +78,18 @@
     hd = tab_ref.shape[2]
     for h in range(qt.shape[0] // hd):
         rows = slice(h * hd, (h + 1) * hd)
-        out_ref[0, rows] = turned(qt[rows], tab_ref[0, 0], tab_ref[0, 1]).astype(BF16)
-
-
-def pair_kernel(hd, q_ref, out_ref):
+        out_ref[rows] = turned(qt[rows], tab_ref[0, 0], tab_ref[0, 1]).astype(BF16)
+
+
+def pair_kernel(hd, zp_ref, q_ref, out_ref):
     n_q, qc, rows = q_ref.shape
-    for i in range(n_q):
-        for h in range(qc // hd):
-            out_ref[i // 2, h, :, (i % 2) * rows : (i % 2 + 1) * rows] = q_ref[
-                i, h * hd : (h + 1) * hd, :
-            ]
+    for i in range(n_q // 2):
+        for b in range(2):
+            block = 2 * i + (zp_ref[0] + b) % 2
+            for h in range(qc // hd):
+                out_ref[i, h, :, b * rows : (b + 1) * rows] = q_ref[
+                    block, h * hd : (h + 1) * hd, :
+                ]
 
 
 def attend_kernel(hd, q_ref, kv_ref, out_ref, k_ref, v_ref):
@@ -173,6 +175,14 @@
     tokens_in, tab = lax.optimization_barrier((tokens_in, tab))
     tokens = to_all(tokens_in, TP).reshape(rows, d)
 
+    query = call(
+        q_kernel,
+        jax.ShapeDtypeStruct((qc, rows), BF16),
+        3,
+        2 * rows * d * qc,
+        2 * d * (rows + qc),
+    )(tokens, w_query, tab)
+    other = lax.ppermute(query, "zp", [(0, 1), (1, 0)])
     kv = call(
         functools.partial(kv_kernel, n_k),
         jax.ShapeDtypeStruct((n_k, 2 * hd, rows), BF16),
@@ -181,22 +191,17 @@
         2 * d * (rows + 2 * hd),
     )(tokens, w_key.T, w_value.T, tab)
     kv = lax.all_to_all(kv, "zq", 0, 0, tiled=True)
-
-    query = call(
-        q_kernel,
-        jax.ShapeDtypeStruct((1, qc, rows), BF16),
-        3,
-        2 * rows * d * qc,
-        2 * d * (rows + qc),
-    )(tokens, w_query, tab)
-    query = lax.all_gather(query, ("zp", "y"), axis=0, tiled=True)
-    query = call(
+    query = lax.all_gather(jnp.stack([query, other]), "y", axis=0, tiled=True)
+    query = pl.pallas_call(
         functools.partial(pair_kernel, hd),
-        jax.ShapeDtypeStruct((n_q // 2, heads, hd, 2 * rows), BF16),
-        1,
-        n_q * qc * rows,
-        4 * n_q * qc * rows,
-    )(query)
+        out_shape=jax.ShapeDtypeStruct((n_q // 2, heads, hd, 2 * rows), BF16),
+        in_specs=[pl.BlockSpec(memory_space=pltpu.SMEM), VMEM],
+        out_specs=VMEM,
+        compiler_params=pltpu.CompilerParams(vmem_limit_bytes=16 * 2**20),
+        cost_estimate=pl.CostEstimate(
+            flops=n_q * qc * rows, bytes_accessed=4 * n_q * qc * rows, transcendentals=0
+        ),
+    )(lax.axis_index("zp").astype(jnp.int32)[None], query)
 
     part = call(
         functools.partial(attend_kernel, hd),
@@ -211,7 +216,7 @@
             pltpu.VMEM((hd + 16, n_k * rows), BF16),
         ),
     )(query, kv)
-    got = lax.all_to_all(part, ("zp", "y"), 0, 0, tiled=True)
+    got = lax.all_to_all(part, ("y", "zp"), 0, 0, tiled=True)
 
     partial = call(
         functools.partial(mix_kernel, hd, n_tp),

time: 108 us -> 98 us (0.907)
  blocking collectives: 80.2 us -> 58.7 us
  waiting for transfers between devices: 0.01 us -> 8.25 us
  starting transfers between devices: 11.2 us -> 13.8 us
    all_gather x1, blocking collectives: 26.4 us -> 10.7 us  [body(): query = lax.all_gather(jnp.stack([query, other]), 'y', axis=0, tiled=True)]
    ppermute x0 -> x1, waiting for transfers between devices: none -> 8.25 us  [body(): other = lax.ppermute(query, 'zp', [(0, 1), (1, 0)])]
    all_to_all x1, blocking collectives: 21.4 us -> 17.1 us  [body(): got = lax.all_to_all(partial, TP, 0, 0, tiled=True)]
    ppermute x0 -> x1, starting transfers between devices: none -> 2.65 us  [body(): other = lax.ppermute(query, 'zp', [(0, 1), (1, 0)])]
    all_to_all x1, blocking collectives: 13.7 us -> 12.3 us  [body(): got = lax.all_to_all(part, ('y', 'zp'), 0, 0, tiled=True)]
  transfers between devices with their start and end apart: 1 -> 2, of which waited for: 0 -> 1; matrix products, arithmetic and copies ran while one was open for 0% -> 0% of each run, Pallas kernels for 0% -> 1%
where the time goes in v3:
time: 98 us; the launch traced here: 97.1 us
  blocking collectives  58.7 us (60%)
  Pallas kernels  13.8 us (14%)
  starting transfers between devices  13.8 us (14%)
  waiting for transfers between devices  8.25 us (8%)
  local copies, waits for them, and re-layouts  1.47 us (2%)
    all_to_all x1, blocking collectives, to_all(): lax.all_to_all(jnp.broadcast_to(shard[None], (n, *shard.shape)), axis, 0,...  18.7 us
    all_to_all x1, blocking collectives, body(): got = lax.all_to_all(partial, TP, 0, 0, tiled=True)  17.1 us
    all_to_all x1, blocking collectives, body(): got = lax.all_to_all(part, ('y', 'zp'), 0, 0, tiled=True)  12.3 us
    pallas_call x1, Pallas kernels, body(): call(functools.partial(attend_kernel, hd), jax.ShapeDtypeStruct((n_q, qc...  11.6 us
    all_to_all x1, starting transfers between devices, body(): kv = lax.all_to_all(kv, 'zq', 0, 0, tiled=True)  11.2 us
    all_gather x1, blocking collectives, body(): query = lax.all_gather(jnp.stack([query, other]), 'y', axis=0, tiled=True)  10.7 us
    ppermute x1, waiting for transfers between devices, body(): other = lax.ppermute(query, 'zp', [(0, 1), (1, 0)])  8.25 us
    ppermute x1, starting transfers between devices, body(): other = lax.ppermute(query, 'zp', [(0, 1), (1, 0)])  2.65 us
  transfers between devices with their start and end apart: 2, of which 1 were waited for; matrix products, arithmetic and copies ran while one was open for 0% of the time, Pallas kernels for 1%

profile of v3, /device:TPU:1, one launch (start us, length us, event | category | flops | bytes accessed | tf_op | source)
XLA Modules:
  0.0 97.1 jit_solution(12567739521271965843)
XLA Ops:
  0.1 0.1 multiply_cosine_fusion
  0.2 0.0 copy-start.4
  0.2 0.0 copy-start.5
  0.2 0.6 copy-done.4
  0.9 0.0 copy-done.5
  0.9 0.1 shard_map.73.tab_ref
  1.0 0.7 copy-done.6
  1.8 0.0 copy-start.2
  1.8 0.0 copy-start.3
  1.8 18.7 %all_to_all.20 = bf16[8,16,2048]{2,1,0:T(8,128)(2,1)S(1)} all-to-all(bf16[8,16,2048]{2,1,0:T(8,128)(2,1)S(1)} %broadcast_in_dim.20), channel_id=1, replica_groups=mesh['zq'=8,'zp'=2,'y'=4,'x'=4,'c'=2] {'x','c'}, dimensions={0} | all-to-all | bytes 1048576 | tf_op jit(solution)/shard_map/all_to_all | solution.py:35
  20.5 1.2 %shard_map.76 = bf16[8,128,128]{2,1,0:T(8,128)(2,1)} custom-call(bf16[128,2048]{1,0:T(8,128)(2,1)S(1)} %bitcast.9, bf16[64,2048]{1,0:T(8,128)(2,1)S(1)} %bitcast.12, bf16[64,2048]{1,0:T(8,128)(2,1)S(1)} %bitcast.13, f32[2,2,64,128]{3,2,1,0:T(8,128)S(1)} %shard_map.73.tab_ref), custom_call_target="tpu_custom_call" | custom-call | flops 67108864 | bytes 1048576 | tf_op jit(solution)/shard_map/pallas_call | solution.py:186
  21.7 11.2 %all-to-all-start.1 = ((bf16[8,128,128]{2,1,0:T(8,128)(2,1)}), bf16[8,128,128]{2,1,0:T(8,128)(2,1)S(1)}, u32[]{:S(2)}, u32[]{:S(2)}) async-start(bf16[8,128,128]{2,1,0:T(8,128)(2,1)} %shard_map.76), calls=%async_computation.1 | async-start | bytes 524288 | tf_op jit(solution)/shard_map/all_to_all | solution.py:193
  32.9 0.4 shard_map.74
  33.3 2.6 %collective-permute-start = (bf16[256,128]{1,0:T(8,128)(2,1)S(1)}, bf16[256,128]{1,0:T(8,128)(2,1)S(1)}, u32[]{:S(2)}, u32[]{:S(2)}) collective-permute-start(bf16[256,128]{1,0:T(8,128)(2,1)S(1)} %shard_map.74), channel_id=1, source_target_pairs={{0,32},{32,0},{1,33},{33,1},{2,34},{34,2},{3,35},{35,3},{4,36},{36... | collective-permute-start | bytes 196616 | tf_op jit(solution)/shard_map/ppermute | solution.py:185
  35.9 8.2 %collective-permute-done = bf16[256,128]{1,0:T(8,128)(2,1)S(1)} collective-permute-done((bf16[256,128]{1,0:T(8,128)(2,1)S(1)}, bf16[256,128]{1,0:T(8,128)(2,1)S(1)}, u32[]{:S(2)}, u32[]{:S(2)}) %collective-permute-start) | collective-permute-done | bytes 65568 | tf_op jit(solution)/shard_map/ppermute | solution.py:185
  44.2 10.7 %all_gather.3.q_ref = bf16[8,256,128]{2,1,0:T(8,128)(2,1)S(1)} all-gather(bf16[2,256,128]{2,1,0:T(8,128)(2,1)S(1)} %pad_maximum_fusion), channel_id=1, replica_groups=mesh['zq'=8,'zp'=2,'y'=4,'x'=4,'c'=2] {'y'}, dimensions={0}, use_global_device_ids=true | all-gather | bytes 655360 | tf_op jit(solution)/shard_map/all_gather | solution.py:194
  54.9 0.1 shard_map.75.q_ref
  55.0 0.0 all-to-all-done.1.kv_ref
  55.0 11.6 %shard_map.77 = bf16[8,272,128]{2,1,0:T(8,128)(2,1)S(1)} custom-call(bf16[4,4,64,256]{3,2,1,0:T(8,128)(2,1)S(1)} %shard_map.75.q_ref, bf16[8,128,128]{2,1,0:T(8,128)(2,1)S(1)} %all-to-all-done.1.kv_ref), custom_call_target="tpu_custom_call" | custom-call | flops 1073741824 | bytes 1048576 | tf_op jit(solution)/shard_map/pallas_call | solution.py:206
  66.6 0.0 copy-start.1
  66.6 12.3 %all_to_all.21.got_ref = bf16[8,272,128]{2,1,0:T(8,128)(2,1)S(1)} all-to-all(bf16[8,272,128]{2,1,0:T(8,128)(2,1)S(1)} %shard_map.77), channel_id=1, replica_groups=mesh['zq'=8,'zp'=2,'y'=4,'x'=4,'c'=2] {'y','zp'}, dimensions={0} | all-to-all | bytes 1114112 | tf_op jit(solution)/shard_map/all_to_all | solution.py:219
  78.9 0.4 shard_map.78
  79.4 17.1 %all_to_all.22 = bf16[8,16,2048]{2,1,0:T(8,128)(2,1)S(1)} all-to-all(bf16[8,16,2048]{2,1,0:T(8,128)(2,1)S(1)} %shard_map.78), channel_id=1, replica_groups=mesh['zq'=8,'zp'=2,'y'=4,'x'=4,'c'=2] {'x','c'}, dimensions={0} | all-to-all | bytes 1048576 | tf_op jit(solution)/shard_map/all_to_all | solution.py:229
  96.4 0.7 reduce_sum.12
  (12 shorter events, 0.1 us)
Async XLA Ops:
  0.2 0.7 copy-start.4
  0.2 0.7 copy-start.5
  0.9 0.8 copy-start.6
  1.8 18.7 %copy-start.2 = (bf16[2048,64]{0,1:T(8,128)(2,1)S(1)}, bf16[2048,64]{0,1:T(8,128)(2,1)}, u32[]{:S(2)}) copy-start(bf16[2048,64]{0,1:T(8,128)(2,1)} %param.9) | copy-start | bytes 786436
  1.8 18.7 %copy-start.3 = (bf16[2048,64]{0,1:T(8,128)(2,1)S(1)}, bf16[2048,64]{0,1:T(8,128)(2,1)}, u32[]{:S(2)}) copy-start(bf16[2048,64]{0,1:T(8,128)(2,1)} %param.10) | copy-start | bytes 786436
  20.5 12.4 %copy-start = (bf16[2048,256]{1,0:T(8,128)(2,1)S(1)}, bf16[2048,256]{1,0:T(8,128)(2,1)}, u32[]{:S(2)}) copy-start(bf16[2048,256]{1,0:T(8,128)(2,1)} %w_ref.2) | copy-start | bytes 3145732
  21.7 33.3 %all-to-all-start.1 = ((bf16[8,128,128]{2,1,0:T(8,128)(2,1)}), bf16[8,128,128]{2,1,0:T(8,128)(2,1)S(1)}, u32[]{:S(2)}, u32[]{:S(2)}) async-start(bf16[8,128,128]{2,1,0:T(8,128)(2,1)} %shard_map.76), calls=%async_computation.1 | async-start | bytes 524288 | tf_op jit(solution)/shard_map/all_to_all | solution.py:193
  33.3 10.9 %collective-permute-start = (bf16[256,128]{1,0:T(8,128)(2,1)S(1)}, bf16[256,128]{1,0:T(8,128)(2,1)S(1)}, u32[]{:S(2)}, u32[]{:S(2)}) collective-permute-start(bf16[256,128]{1,0:T(8,128)(2,1)S(1)} %shard_map.74), channel_id=1, source_target_pairs={{0,32},{32,0},{1,33},{33,1},{2,34},{34,2},{3,35},{35,3},{4,36},{36... | collective-permute-start | bytes 196616 | tf_op jit(solution)/shard_map/ppermute | solution.py:185
  66.6 12.3 %copy-start.1 = (bf16[256,2048]{1,0:T(8,128)(2,1)S(1)}, bf16[256,2048]{1,0:T(8,128)(2,1)}, u32[]{:S(2)}) copy-start(bf16[256,2048]{1,0:T(8,128)(2,1)} %w_ref.3) | copy-start | bytes 3145732

commit v4 on v3

--- a/solution.py
+++ b/solution.py
@@ -30,25 +30,17 @@
     )
 
 
-def to_all(shard, axis):
-    n = lax.axis_size(axis)
-    return lax.all_to_all(
-        jnp.broadcast_to(shard[None], (n, *shard.shape)), axis, 0, 0, tiled=True
-    )
-
-
-def table_kernel(qg_ref, kg_ref, tab_ref, out_ref):
+def tables(gain, tab_ref):
     p = tab_ref.shape[1]
-    for i, ref in enumerate((qg_ref, kg_ref)):
-        gain = jnp.broadcast_to(ref[...], (tab_ref.shape[2], ref.shape[1])).T
-        for half in range(2):
-            cos, sin = tab_ref[2 * half], tab_ref[2 * half + 1]
-            a, b = 2 * half * p, (2 * half + 1) * p
-            ga, gb = gain[a : a + p], gain[b : b + p]
-            out_ref[i, 0, a : a + p] = ga * cos
-            out_ref[i, 0, b : b + p] = gb * cos
-            out_ref[i, 1, a : a + p] = -gb * sin
-            out_ref[i, 1, b : b + p] = ga * sin
+    gain = jnp.broadcast_to(gain, (tab_ref.shape[2], gain.shape[1])).T
+    cosines, sines = [], []
+    for half in range(2):
+        cos, sin = tab_ref[2 * half], tab_ref[2 * half + 1]
+        ga = gain[2 * half * p : (2 * half + 1) * p]
+        gb = gain[(2 * half + 1) * p : (2 * half + 2) * p]
+        cosines += [ga * cos, gb * cos]
+        sines += [-gb * sin, ga * sin]
+    return jnp.concatenate(cosines, axis=0), jnp.concatenate(sines, axis=0)
 
 
 def turned(u, cos, sin):
@@ -62,23 +54,29 @@
 NT = (((1,), (1,)), ((), ()))
 
 
-def kv_kernel(copies, x_ref, wk_ref, wv_ref, tab_ref, out_ref):
-    x = x_ref[...]
+def in_order(x_ref):
+    n = x_ref.shape[0]
+    return jnp.concatenate([x_ref[(t % 2) * (n // 2) + t // 2] for t in range(n)], axis=0)
+
+
+def kv_kernel(copies, x_ref, wk_ref, wv_ref, gain_ref, tab_ref, out_ref):
+    x = in_order(x_ref)
     k = lax.dot_general(wk_ref[...], x, NT, preferred_element_type=F32)
     v = lax.dot_general(wv_ref[...], x, NT, preferred_element_type=F32)
-    kt = turned(k.astype(BF16).astype(F32), tab_ref[1, 0], tab_ref[1, 1]).astype(BF16)
+    kt = turned(k.astype(BF16).astype(F32), *tables(gain_ref[1:2], tab_ref)).astype(BF16)
     both = jnp.concatenate([kt, v.astype(BF16)], axis=0)
     for i in range(copies):
         out_ref[i] = both
 
 
-def q_kernel(x_ref, w_ref, tab_ref, out_ref):
-    q = jnp.dot(x_ref[...], w_ref[...], preferred_element_type=F32)
+def q_kernel(x_ref, w_ref, gain_ref, tab_ref, out_ref):
+    q = jnp.dot(in_order(x_ref), w_ref[...], preferred_element_type=F32)
     qt = q.astype(BF16).astype(F32).T
-    hd = tab_ref.shape[2]
+    hd = gain_ref.shape[1]
+    both = tables(gain_ref[0:1], tab_ref)
     for h in range(qt.shape[0] // hd):
         rows = slice(h * hd, (h + 1) * hd)
-        out_ref[rows] = turned(qt[rows], tab_ref[0, 0], tab_ref[0, 1]).astype(BF16)
+        out_ref[rows] = turned(qt[rows], *both).astype(BF16)
 
 
 def pair_kernel(hd, zp_ref, q_ref, out_ref):
@@ -92,38 +90,54 @@
                 ]
 
 
-def attend_kernel(hd, q_ref, kv_ref, out_ref, k_ref, v_ref):
+def attend_kernel(hd, q_ref, kv_ref, out_ref, k_ref, v_ref, s_ref):
     n_pair, heads, _, rows = q_ref.shape
     rows //= 2
     n_k = kv_ref.shape[0]
+    n_keys = n_k * rows
     qc = heads * hd
+    step = n_keys // 2
     scale = hd**-0.5 * LOG2E
     for j in range(n_k):
         k_ref[j * rows : (j + 1) * rows, :] = kv_ref[j, :hd, :].astype(F32).T.astype(BF16)
         v_ref[16:, j * rows : (j + 1) * rows] = kv_ref[j, hd:, :]
-    v_ref[:16, :] = jnp.ones((16, n_k * rows), BF16)
-
-    def pair(i, _):
+    v_ref[:16, :] = jnp.ones((16, n_keys), BF16)
+
+    def score(i, h, slot):
+        top = None
+        for c in range(0, n_keys, step):
+            s = jnp.dot(k_ref[c : c + step, :], q_ref[i, h], preferred_element_type=F32)
+            s_ref[slot, c : c + step] = s
+            part = jnp.max(s.reshape(step // 8, 8, 2 * rows), axis=0)
+            top = part if top is None else jnp.maximum(top, part)
+        return (jnp.max(top, axis=0, keepdims=True) * scale).astype(BF16).astype(F32)
+
+    def pair(i, top):
         tops, sums = [], []
         for h in range(heads):
-            s = jnp.dot(k_ref[...], q_ref[i, h], preferred_element_type=F32)
-            top = (jnp.max(s, axis=0, keepdims=True) * scale).astype(BF16).astype(F32)
-            p = jnp.exp2(s * scale - top).astype(BF16)
-            o = jnp.dot(v_ref[...], p, preferred_element_type=F32)
+            if h + 1 < heads:
+                later = score(i, h + 1, (h + 1) % 2)
+            else:
+                later = score(jnp.minimum(i + 1, n_pair - 1), 0, 0)
+            o = 0.0
+            for c in range(0, n_keys, step):
+                p = jnp.exp2(s_ref[h % 2, c : c + step] * scale - top).astype(BF16)
+                o += jnp.dot(v_ref[:, c : c + step], p, preferred_element_type=F32)
             tops.append(top)
             sums.append(o[:1])
             for b in range(2):
                 out_ref[2 * i + b, h * hd : (h + 1) * hd, :] = o[
                     16:, b * rows : (b + 1) * rows
                 ].astype(BF16)
+            top = later
         total = jnp.concatenate(sums, axis=0)
         hi = total.astype(BF16).astype(F32)
         stats = jnp.concatenate(tops + [hi, total - hi, jnp.zeros_like(total)], axis=0).astype(BF16)
         for b in range(2):
             out_ref[2 * i + b, qc:, :] = stats[:, b * rows : (b + 1) * rows]
-        return 0
-
-    lax.fori_loop(0, n_pair, pair, 0)
+        return top
+
+    lax.fori_loop(0, n_pair, pair, score(0, 0, 0))
 
 
 def mix_kernel(hd, n_tp, got_ref, w_ref, out_ref, mixed_ref):
@@ -165,31 +179,27 @@
     grid = jnp.stack([position // GRID_W, position % GRID_W]).astype(F32)
     angle = grid[:, None, :] * freq[None, :, None]
     tab = jnp.stack([jnp.cos(angle), jnp.sin(angle)], axis=1).reshape(4, pairs, rows)
-    tab = call(
-        table_kernel,
-        jax.ShapeDtypeStruct((2, 2, hd, rows), F32),
-        3,
-        8 * hd * rows,
-        32 * hd * rows,
-    )(q_gain[None], k_gain[None], tab)
-    tokens_in, tab = lax.optimization_barrier((tokens_in, tab))
-    tokens = to_all(tokens_in, TP).reshape(rows, d)
+    gains = jnp.stack([q_gain, k_gain])
+    tokens_in, tab, gains = lax.optimization_barrier((tokens_in, tab, gains))
+    sent = jnp.broadcast_to(tokens_in[None], (lax.axis_size("x"), mine, d))
+    tokens = lax.all_to_all(sent, "x", 0, 0, tiled=True)
+    tokens = lax.all_gather(tokens, "c", axis=0).reshape(n_tp, mine, d)
 
     query = call(
         q_kernel,
         jax.ShapeDtypeStruct((qc, rows), BF16),
-        3,
+        4,
         2 * rows * d * qc,
         2 * d * (rows + qc),
-    )(tokens, w_query, tab)
+    )(tokens, w_query, gains, tab)
     other = lax.ppermute(query, "zp", [(0, 1), (1, 0)])
     kv = call(
         functools.partial(kv_kernel, n_k),
         jax.ShapeDtypeStruct((n_k, 2 * hd, rows), BF16),
-        4,
+        5,
         2 * rows * d * 2 * hd,
         2 * d * (rows + 2 * hd),
-    )(tokens, w_key.T, w_value.T, tab)
+    )(tokens, w_key.T, w_value.T, gains, tab)
     kv = lax.all_to_all(kv, "zq", 0, 0, tiled=True)
     query = lax.all_gather(jnp.stack([query, other]), "y", axis=0, tiled=True)
     query = pl.pallas_call(
@@ -214,6 +224,7 @@
         scratch=(
             pltpu.VMEM((n_k * rows, hd), BF16),
             pltpu.VMEM((hd + 16, n_k * rows), BF16),
+            pltpu.VMEM((2, n_k * rows, 2 * rows), F32),
         ),
     )(query, kv)
     got = lax.all_to_all(part, ("y", "zp"), 0, 0, tiled=True)

time: 98 us -> 89.6 us (0.914)
  Pallas kernels: 13.8 us -> 6.88 us
    all_to_all x1, blocking collectives: 18.7 us -> 10.2 us  [body(): tokens = lax.all_to_all(sent, 'x', 0, 0, tiled=True)]
    all_gather x0 -> x1, blocking collectives: none -> 7.67 us  [body(): tokens = lax.all_gather(tokens, 'c', axis=0).reshape(n_tp, mine, d)]
    pallas_call x1, Pallas kernels: 11.6 us -> 4.71 us  [body(): call(functools.partial(attend_kernel, hd), jax.ShapeDtypeStruct((n_q, qc...]
where the time goes in v4:
time: 89.6 us; the launch traced here: 88.7 us
  blocking collectives  58.1 us (65%)
  starting transfers between devices  13.8 us (15%)
  waiting for transfers between devices  8.2 us (9%)
  Pallas kernels  6.88 us (8%)
  other arithmetic  0.9 us (1%)
    all_to_all x1, blocking collectives, body(): got = lax.all_to_all(partial, TP, 0, 0, tiled=True)  17.1 us
    all_to_all x1, blocking collectives, body(): got = lax.all_to_all(part, ('y', 'zp'), 0, 0, tiled=True)  12.2 us
    all_to_all x1, starting transfers between devices, body(): kv = lax.all_to_all(kv, 'zq', 0, 0, tiled=True)  11.2 us
    all_gather x1, blocking collectives, body(): query = lax.all_gather(jnp.stack([query, other]), 'y', axis=0, tiled=True)  11 us
    all_to_all x1, blocking collectives, body(): tokens = lax.all_to_all(sent, 'x', 0, 0, tiled=True)  10.2 us
    ppermute x1, waiting for transfers between devices, body(): other = lax.ppermute(query, 'zp', [(0, 1), (1, 0)])  8.2 us
    all_gather x1, blocking collectives, body(): tokens = lax.all_gather(tokens, 'c', axis=0).reshape(n_tp, mine, d)  7.67 us
    pallas_call x1, Pallas kernels, body(): call(functools.partial(attend_kernel, hd), jax.ShapeDtypeStruct((n_q, qc...  4.71 us
  transfers between devices with their start and end apart: 2, of which 1 were waited for; matrix products, arithmetic and copies ran while one was open for 0% of the time, Pallas kernels for 1%

profile of v4, /device:TPU:1, one launch (start us, length us, event | category | flops | bytes accessed | tf_op | source)
XLA Modules:
  0.0 88.7 jit_solution(13598191867364209738)
XLA Ops:
  0.0 0.0 copy-start.5
  0.0 0.0 copy-start.6
  0.0 0.0 copy-start.4
  0.1 0.6 copy-done.5
  0.7 0.0 copy-done.6
  0.7 0.1 multiply_cosine_fusion
  0.9 0.0 copy-done.4
  0.9 10.2 %all_to_all.20 = bf16[4,16,2048]{2,1,0:T(8,128)(2,1)S(1)} all-to-all(bf16[4,16,2048]{2,1,0:T(8,128)(2,1)S(1)} %broadcast_in_dim.5), channel_id=1, replica_groups=mesh['zq'=8,'zp'=2,'y'=4,'x'=4,'c'=2] {'x'}, dimensions={0} | all-to-all | bytes 524288 | tf_op jit(solution)/shard_map/all_to_all | solution.py:185
  11.1 7.7 %all-gather.x_ref = bf16[8,16,2048]{2,1,0:T(8,128)(2,1)S(1)} all-gather(bf16[4,16,2048]{2,1,0:T(8,128)(2,1)S(1)} %all_to_all.20), channel_id=2, replica_groups=mesh['zq'=8,'zp'=2,'y'=4,'x'=4,'c'=2] {'c'}, dimensions={0}, use_global_device_ids=true | all-gather | bytes 786432 | tf_op jit(solution)/shard_map/all_gather | solution.py:186
  18.7 0.0 copy-done.3
  18.8 1.2 %shard_map.75 = bf16[8,128,128]{2,1,0:T(8,128)(2,1)} custom-call(bf16[8,16,2048]{2,1,0:T(8,128)(2,1)S(1)} %all-gather.x_ref, bf16[64,2048]{1,0:T(8,128)(2,1)S(1)} %bitcast.11, bf16[64,2048]{1,0:T(8,128)(2,1)S(1)} %bitcast.12, f32[2,64]{1,0:T(2,128)S(1)} %pad_maximum_fusion.2.gain_ref, f32[4,16,128]{2,1,0:T(8,128)S(1)} %bitcast.8), custom_call_target="tpu_custom_call" | custom-call | flops 67108864 | bytes 1048576 | tf_op jit(solution)/shard_map/pallas_call | solution.py:196
  20.0 11.2 %all-to-all-start.1 = ((bf16[8,128,128]{2,1,0:T(8,128)(2,1)}), bf16[8,128,128]{2,1,0:T(8,128)(2,1)S(1)}, u32[]{:S(2)}, u32[]{:S(2)}) async-start(bf16[8,128,128]{2,1,0:T(8,128)(2,1)} %shard_map.75), calls=%async_computation.1 | async-start | bytes 524288 | tf_op jit(solution)/shard_map/all_to_all | solution.py:203
  31.1 0.4 shard_map.73
  31.6 2.6 %collective-permute-start = (bf16[256,128]{1,0:T(8,128)(2,1)S(1)}, bf16[256,128]{1,0:T(8,128)(2,1)S(1)}, u32[]{:S(2)}, u32[]{:S(2)}) collective-permute-start(bf16[256,128]{1,0:T(8,128)(2,1)S(1)} %shard_map.73), channel_id=1, source_target_pairs={{0,32},{32,0},{1,33},{33,1},{2,34},{34,2},{3,35},{35,3},{4,36},{36... | collective-permute-start | bytes 196616 | tf_op jit(solution)/shard_map/ppermute | solution.py:195
  34.2 8.2 %collective-permute-done = bf16[256,128]{1,0:T(8,128)(2,1)S(1)} collective-permute-done((bf16[256,128]{1,0:T(8,128)(2,1)S(1)}, bf16[256,128]{1,0:T(8,128)(2,1)S(1)}, u32[]{:S(2)}, u32[]{:S(2)}) %collective-permute-start) | collective-permute-done | bytes 65568 | tf_op jit(solution)/shard_map/ppermute | solution.py:195
  42.4 11.0 %all_gather.11.q_ref = bf16[8,256,128]{2,1,0:T(8,128)(2,1)S(1)} all-gather(bf16[2,256,128]{2,1,0:T(8,128)(2,1)S(1)} %pad_maximum_fusion), channel_id=1, replica_groups=mesh['zq'=8,'zp'=2,'y'=4,'x'=4,'c'=2] {'y'}, dimensions={0}, use_global_device_ids=true | all-gather | bytes 655360 | tf_op jit(solution)/shard_map/all_gather | solution.py:204
  53.5 0.1 shard_map.74.q_ref
  53.6 0.0 all-to-all-done.1.kv_ref
  53.6 4.7 %shard_map.76 = bf16[8,272,128]{2,1,0:T(8,128)(2,1)S(1)} custom-call(bf16[4,4,64,256]{3,2,1,0:T(8,128)(2,1)S(1)} %shard_map.74.q_ref, bf16[8,128,128]{2,1,0:T(8,128)(2,1)S(1)} %all-to-all-done.1.kv_ref), custom_call_target="tpu_custom_call" | custom-call | flops 1073741824 | bytes 1048576 | tf_op jit(solution)/shard_map/pallas_call | solution.py:216
  58.3 0.0 copy-start.1
  58.3 12.2 %all_to_all.21.got_ref = bf16[8,272,128]{2,1,0:T(8,128)(2,1)S(1)} all-to-all(bf16[8,272,128]{2,1,0:T(8,128)(2,1)S(1)} %shard_map.76), channel_id=1, replica_groups=mesh['zq'=8,'zp'=2,'y'=4,'x'=4,'c'=2] {'y','zp'}, dimensions={0} | all-to-all | bytes 1114112 | tf_op jit(solution)/shard_map/all_to_all | solution.py:230
  70.5 0.4 shard_map.77
  70.9 17.1 %all_to_all.22 = bf16[8,16,2048]{2,1,0:T(8,128)(2,1)S(1)} all-to-all(bf16[8,16,2048]{2,1,0:T(8,128)(2,1)S(1)} %shard_map.77), channel_id=1, replica_groups=mesh['zq'=8,'zp'=2,'y'=4,'x'=4,'c'=2] {'x','c'}, dimensions={0} | all-to-all | bytes 1048576 | tf_op jit(solution)/shard_map/all_to_all | solution.py:240
  88.0 0.7 reduce_sum.12
  (13 shorter events, 0.1 us)
Async XLA Ops:
  0.0 0.7 copy-start.5
  0.0 0.7 copy-start.6
  0.0 0.8 copy-start.4
  11.1 7.7 %copy-start.2 = (bf16[2048,64]{0,1:T(8,128)(2,1)S(1)}, bf16[2048,64]{0,1:T(8,128)(2,1)}, u32[]{:S(2)}) copy-start(bf16[2048,64]{0,1:T(8,128)(2,1)} %param.9) | copy-start | bytes 786436
  11.1 7.7 %copy-start.3 = (bf16[2048,64]{0,1:T(8,128)(2,1)S(1)}, bf16[2048,64]{0,1:T(8,128)(2,1)}, u32[]{:S(2)}) copy-start(bf16[2048,64]{0,1:T(8,128)(2,1)} %param.10) | copy-start | bytes 786436
  18.7 12.4 %copy-start = (bf16[2048,256]{1,0:T(8,128)(2,1)S(1)}, bf16[2048,256]{1,0:T(8,128)(2,1)}, u32[]{:S(2)}) copy-start(bf16[2048,256]{1,0:T(8,128)(2,1)} %w_ref.2) | copy-start | bytes 3145732
  20.0 33.6 %all-to-all-start.1 = ((bf16[8,128,128]{2,1,0:T(8,128)(2,1)}), bf16[8,128,128]{2,1,0:T(8,128)(2,1)S(1)}, u32[]{:S(2)}, u32[]{:S(2)}) async-start(bf16[8,128,128]{2,1,0:T(8,128)(2,1)} %shard_map.75), calls=%async_computation.1 | async-start | bytes 524288 | tf_op jit(solution)/shard_map/all_to_all | solution.py:203
  31.6 10.8 %collective-permute-start = (bf16[256,128]{1,0:T(8,128)(2,1)S(1)}, bf16[256,128]{1,0:T(8,128)(2,1)S(1)}, u32[]{:S(2)}, u32[]{:S(2)}) collective-permute-start(bf16[256,128]{1,0:T(8,128)(2,1)S(1)} %shard_map.73), channel_id=1, source_target_pairs={{0,32},{32,0},{1,33},{33,1},{2,34},{34,2},{3,35},{35,3},{4,36},{36... | collective-permute-start | bytes 196616 | tf_op jit(solution)/shard_map/ppermute | solution.py:195
  58.3 12.2 %copy-start.1 = (bf16[256,2048]{1,0:T(8,128)(2,1)S(1)}, bf16[256,2048]{1,0:T(8,128)(2,1)}, u32[]{:S(2)}) copy-start(bf16[256,2048]{1,0:T(8,128)(2,1)} %w_ref.3) | copy-start | bytes 3145732

commit v5 on v4

--- a/solution.py
+++ b/solution.py
@@ -54,13 +54,8 @@
 NT = (((1,), (1,)), ((), ()))
 
 
-def in_order(x_ref):
-    n = x_ref.shape[0]
-    return jnp.concatenate([x_ref[(t % 2) * (n // 2) + t // 2] for t in range(n)], axis=0)
-
-
 def kv_kernel(copies, x_ref, wk_ref, wv_ref, gain_ref, tab_ref, out_ref):
-    x = in_order(x_ref)
+    x = x_ref[...]
     k = lax.dot_general(wk_ref[...], x, NT, preferred_element_type=F32)
     v = lax.dot_general(wv_ref[...], x, NT, preferred_element_type=F32)
     kt = turned(k.astype(BF16).astype(F32), *tables(gain_ref[1:2], tab_ref)).astype(BF16)
@@ -70,7 +65,7 @@
 
 
 def q_kernel(x_ref, w_ref, gain_ref, tab_ref, out_ref):
-    q = jnp.dot(in_order(x_ref), w_ref[...], preferred_element_type=F32)
+    q = jnp.dot(x_ref[...], w_ref[...], preferred_element_type=F32)
     qt = q.astype(BF16).astype(F32).T
     hd = gain_ref.shape[1]
     both = tables(gain_ref[0:1], tab_ref)
@@ -95,7 +90,6 @@
     rows //= 2
     n_k = kv_ref.shape[0]
     n_keys = n_k * rows
-    qc = heads * hd
     step = n_keys // 2
     scale = hd**-0.5 * LOG2E
     for j in range(n_k):
@@ -112,8 +106,16 @@
             top = part if top is None else jnp.maximum(top, part)
         return (jnp.max(top, axis=0, keepdims=True) * scale).astype(BF16).astype(F32)
 
+    left = lax.broadcasted_iota(jnp.int32, (1, rows), 1) < rows // 2
+
+    def halves(a, b):
+        return (
+            jnp.where(left, a, pltpu.roll(b, rows // 2, 1)),
+            jnp.where(left, pltpu.roll(a, rows // 2, 1), b),
+        )
+
     def pair(i, top):
-        tops, sums = [], []
+        outs, tops, sums = [], [], []
         for h in range(heads):
             if h + 1 < heads:
                 later = score(i, h + 1, (h + 1) % 2)
@@ -123,44 +125,57 @@
             for c in range(0, n_keys, step):
                 p = jnp.exp2(s_ref[h % 2, c : c + step] * scale - top).astype(BF16)
                 o += jnp.dot(v_ref[:, c : c + step], p, preferred_element_type=F32)
+            outs.append(o[16:])
+            sums.append(o[:1])
             tops.append(top)
-            sums.append(o[:1])
-            for b in range(2):
-                out_ref[2 * i + b, h * hd : (h + 1) * hd, :] = o[
-                    16:, b * rows : (b + 1) * rows
-                ].astype(BF16)
             top = later
         total = jnp.concatenate(sums, axis=0)
         hi = total.astype(BF16).astype(F32)
-        stats = jnp.concatenate(tops + [hi, total - hi, jnp.zeros_like(total)], axis=0).astype(BF16)
+        lo = total - hi
+        tops = jnp.concatenate(tops, axis=0)
+        n = heads // 2
         for b in range(2):
-            out_ref[2 * i + b, qc:, :] = stats[:, b * rows : (b + 1) * rows]
+            lanes = slice(b * rows, (b + 1) * rows)
+            for h in range(n):
+                for c, part in enumerate(halves(outs[h][:, lanes], outs[h + n][:, lanes])):
+                    out_ref[4 * i + 2 * b + c, h * hd : (h + 1) * hd, :] = part.astype(BF16)
+            stats = [halves(r[:n, lanes], r[n:, lanes]) for r in (tops, hi, lo)]
+            for c in range(2):
+                both = [r[c] for r in stats] + [jnp.zeros((16 - 3 * n, rows), F32)]
+                out_ref[4 * i + 2 * b + c, n * hd :, :] = jnp.concatenate(both, axis=0).astype(BF16)
         return top
 
     lax.fori_loop(0, n_pair, pair, score(0, 0, 0))
 
 
-def mix_kernel(hd, n_tp, got_ref, w_ref, out_ref, mixed_ref):
-    parts, _, rows = got_ref.shape
-    qc = w_ref.shape[0]
-    heads = qc // hd
-    st = [got_ref[i, qc:, :].astype(F32) for i in range(parts)]
-    top = functools.reduce(jnp.maximum, [s[:heads] for s in st])
-    factor = [jnp.exp2(s[:heads] - top) for s in st]
-    total = functools.reduce(
-        jnp.add,
-        [f * (s[heads : 2 * heads] + s[2 * heads : 3 * heads]) for f, s in zip(factor, st)],
-    )
-    for h in range(heads):
-        acc = 0.0
-        for i in range(parts):
-            acc += got_ref[i, h * hd : (h + 1) * hd, :].astype(F32) * factor[i][h : h + 1]
-        mixed_ref[h * hd : (h + 1) * hd, :] = acc / total[h : h + 1]
-    mixed = mixed_ref[...].T.astype(BF16)
-    out = jnp.dot(mixed, w_ref[...], preferred_element_type=F32).astype(BF16)
-    each = rows // n_tp
-    for t in range(n_tp):
-        out_ref[t] = out[t * each : (t + 1) * each]
+def mix_kernel(hd, core_ref, got_ref, own_ref, other_ref, out_ref):
+    parts = got_ref.shape[0] // 2
+    rows = got_ref.shape[2]
+    n = own_ref.shape[0] // hd // 2
+    far, mine, _ = out_ref.shape
+
+    def mixed(core):
+        st = [got_ref[2 * i + core, n * hd :, :].astype(F32) for i in range(parts)]
+        top = functools.reduce(jnp.maximum, [s[:n] for s in st])
+        factor = [jnp.exp2(s[:n] - top) for s in st]
+        total = functools.reduce(
+            jnp.add, [f * (s[n : 2 * n] + s[2 * n : 3 * n]) for f, s in zip(factor, st)]
+        )
+        heads = []
+        for h in range(n):
+            acc = 0.0
+            for i in range(parts):
+                acc += got_ref[2 * i + core, h * hd : (h + 1) * hd, :].astype(F32) * factor[i][h : h + 1]
+            heads.append(acc / total[h : h + 1])
+        turned_round = jnp.concatenate(heads, axis=0).T
+        half = rows // 2
+        return jnp.concatenate([turned_round[:half], turned_round[half:]], axis=1).astype(BF16)
+
+    core = core_ref[0]
+    out = jnp.dot(mixed(core), own_ref[...], preferred_element_type=F32)
+    out += jnp.dot(mixed(1 - core), other_ref[...], preferred_element_type=F32)
+    for x in range(far):
+        out_ref[x] = out[x * mine : (x + 1) * mine].astype(BF16)
 
 
 def body(tokens_in, w_query, w_key, w_value, w_out, q_gain, k_gain):
@@ -173,7 +188,10 @@
     n_q = lax.axis_size(("zp", "y"))
     heads = qc // hd
 
-    position = lax.axis_index(SP) * rows + jnp.arange(rows, dtype=jnp.int32)
+    n_x, n_c = lax.axis_size("x"), lax.axis_size("c")
+    lane = jnp.arange(rows, dtype=jnp.int32)
+    core_of, x_of, row_of = lane // (n_x * mine), lane // mine % n_x, lane % mine
+    position = lax.axis_index(SP) * rows + (x_of * n_c + core_of) * mine + row_of
     pairs = hd // 4
     freq = 10000.0 ** (-jnp.arange(pairs, dtype=F32) / pairs)
     grid = jnp.stack([position // GRID_W, position % GRID_W]).astype(F32)
@@ -183,7 +201,7 @@
     tokens_in, tab, gains = lax.optimization_barrier((tokens_in, tab, gains))
     sent = jnp.broadcast_to(tokens_in[None], (lax.axis_size("x"), mine, d))
     tokens = lax.all_to_all(sent, "x", 0, 0, tiled=True)
-    tokens = lax.all_gather(tokens, "c", axis=0).reshape(n_tp, mine, d)
+    tokens = lax.all_gather(tokens, "c", axis=0).reshape(rows, d)
 
     query = call(
         q_kernel,
@@ -201,6 +219,7 @@
         2 * d * (rows + 2 * hd),
     )(tokens, w_key.T, w_value.T, gains, tab)
     kv = lax.all_to_all(kv, "zq", 0, 0, tiled=True)
+    w_other = lax.ppermute(w_out, "c", [(0, 1), (1, 0)])
     query = lax.all_gather(jnp.stack([query, other]), "y", axis=0, tiled=True)
     query = pl.pallas_call(
         functools.partial(pair_kernel, hd),
@@ -213,9 +232,11 @@
         ),
     )(lax.axis_index("zp").astype(jnp.int32)[None], query)
 
+    core = lax.axis_index("c").astype(jnp.int32)[None]
+    query, w_other, core = lax.optimization_barrier((query, w_other, core))
     part = call(
         functools.partial(attend_kernel, hd),
-        jax.ShapeDtypeStruct((n_q, qc + 16, rows), BF16),
+        jax.ShapeDtypeStruct((2 * n_q, qc // 2 + 16, rows), BF16),
         2,
         4 * heads * n_q * rows * n_k * rows * hd,
         4 * n_q * qc * rows,
@@ -227,17 +248,19 @@
             pltpu.VMEM((2, n_k * rows, 2 * rows), F32),
         ),
     )(query, kv)
-    got = lax.all_to_all(part, ("y", "zp"), 0, 0, tiled=True)
-
-    partial = call(
-        functools.partial(mix_kernel, hd, n_tp),
-        jax.ShapeDtypeStruct((n_tp, mine, d), BF16),
-        2,
-        2 * rows * qc * d,
-        2 * d * (rows + qc),
-        scratch=(pltpu.VMEM((qc, rows), F32),),
-    )(got, w_out)
-    got = lax.all_to_all(partial, TP, 0, 0, tiled=True)
+    got = lax.all_to_all(part, ("y", "zp", "c"), 0, 0, tiled=True)
+
+    partial = pl.pallas_call(
+        functools.partial(mix_kernel, hd),
+        out_shape=jax.ShapeDtypeStruct((n_x, mine, d), BF16),
+        in_specs=[pl.BlockSpec(memory_space=pltpu.SMEM)] + [VMEM] * 3,
+        out_specs=VMEM,
+        compiler_params=pltpu.CompilerParams(vmem_limit_bytes=16 * 2**20),
+        cost_estimate=pl.CostEstimate(
+            flops=2 * rows * qc * d, bytes_accessed=4 * d * qc, transcendentals=0
+        ),
+    )(core, got, w_out, w_other)
+    got = lax.all_to_all(partial, "x", 0, 0, tiled=True)
     return got.astype(F32).sum(axis=0).astype(BF16)
 
 

time: 89.6 us -> 90.3 us (level)
  blocking collectives: 58.1 us -> 45.7 us
  starting transfers between devices: 13.8 us -> 25.3 us
    all_to_all x3 -> x2, blocking collectives: 39.4 us -> 28.3 us  [the longest x1 19.6 us: body(): got = lax.all_to_all(part, ('y', 'zp', 'c'), 0, 0, tiled=True)]
    ppermute x0 -> x1, starting transfers between devices: none -> 7.48 us  [body(): w_other = lax.ppermute(w_out, 'c', [(0, 1), (1, 0)])]
    all_to_all x0 -> x1, starting transfers between devices: none -> 4.83 us  [body(): tokens = lax.all_to_all(sent, 'x', 0, 0, tiled=True)]
    all_gather x1, blocking collectives: 7.67 us -> 6.35 us  [body(): tokens = lax.all_gather(tokens, 'c', axis=0).reshape(rows, d)]
  transfers between devices with their start and end apart: 2 -> 4, of which waited for: 1 -> 1; matrix products, arithmetic and copies ran while one was open for 0% -> 0% of each run, Pallas kernels for 1% -> 2%
where the time goes in v5:
time: 90.3 us; the launch traced here: 89 us
  blocking collectives  45.7 us (51%)
  starting transfers between devices  25.3 us (28%)
  waiting for transfers between devices  8.22 us (9%)
  Pallas kernels  7.37 us (8%)
  local copies, waits for them, and re-layouts  1.38 us (2%)
    all_to_all x1, blocking collectives, body(): got = lax.all_to_all(part, ('y', 'zp', 'c'), 0, 0, tiled=True)  19.6 us
    all_gather x1, blocking collectives, body(): query = lax.all_gather(jnp.stack([query, other]), 'y', axis=0, tiled=True)  11 us
    all_to_all x1, starting transfers between devices, body(): kv = lax.all_to_all(kv, 'zq', 0, 0, tiled=True)  10.4 us
    all_to_all x1, blocking collectives, body(): got = lax.all_to_all(partial, 'x', 0, 0, tiled=True)  8.72 us
    ppermute x1, waiting for transfers between devices, body(): other = lax.ppermute(query, 'zp', [(0, 1), (1, 0)])  8.21 us
    ppermute x1, starting transfers between devices, body(): w_other = lax.ppermute(w_out, 'c', [(0, 1), (1, 0)])  7.48 us
    all_gather x1, blocking collectives, body(): tokens = lax.all_gather(tokens, 'c', axis=0).reshape(rows, d)  6.35 us
    pallas_call x1, Pallas kernels, body(): call(functools.partial(attend_kernel, hd), jax.ShapeDtypeStruct((2 * n_q,...  5.06 us
  transfers between devices with their start and end apart: 4, of which 1 were waited for; matrix products, arithmetic and copies ran while one was open for 0% of the time, Pallas kernels for 2%

profile of v5, /device:TPU:1, one launch (start us, length us, event | category | flops | bytes accessed | tf_op | source)
XLA Modules:
  0.0 89.0 jit_solution(4811779295101071113)
XLA Ops:
  0.0 0.0 copy-start.5
  0.0 0.0 copy-start.6
  0.0 0.0 copy-start.4
  0.1 0.6 copy-done.5
  0.7 0.0 copy-done.6
  0.7 0.1 multiply_cosine_fusion
  0.9 0.0 copy-done.4
  0.9 0.7 broadcast_in_dim.7
  1.6 4.8 %all-to-all-start = ((bf16[4,16,2048]{2,1,0:T(8,128)(2,1)}), bf16[4,16,2048]{2,1,0:T(8,128)(2,1)S(1)}, u32[]{:S(2)}, u32[]{:S(2)}) async-start(bf16[4,16,2048]{2,1,0:T(8,128)(2,1)} %broadcast_in_dim.7), calls=%async_computation | async-start | bytes 524288 | tf_op jit(solution)/shard_map/all_to_all | solution.py:203
  6.4 7.5 %collective-permute-start.1 = (bf16[256,2048]{1,0:T(8,128)(2,1)}, bf16[256,2048]{1,0:T(8,128)(2,1)S(1)}, u32[]{:S(2)}, u32[]{:S(2)}) collective-permute-start(bf16[256,2048]{1,0:T(8,128)(2,1)} %own_ref.1), channel_id=1, source_target_pairs={{0,1},{1,0},{2,3},{3,2},{4,5},{5,4},{6,7},{7,6},{8,9},{9,8},{10,11... | collective-permute-start | bytes 3145736 | tf_op jit(solution)/shard_map/ppermute | solution.py:222
  13.9 6.4 %all-gather = bf16[8,16,2048]{2,1,0:T(8,128)(2,1)S(1)} all-gather(bf16[4,16,2048]{2,1,0:T(8,128)(2,1)S(1)} %all-to-all-done), channel_id=2, replica_groups=mesh['zq'=8,'zp'=2,'y'=4,'x'=4,'c'=2] {'c'}, dimensions={0}, use_global_device_ids=true | all-gather | bytes 786432 | tf_op jit(solution)/shard_map/all_gather | solution.py:204
  20.3 1.2 %shard_map.75 = bf16[8,128,128]{2,1,0:T(8,128)(2,1)} custom-call(bf16[128,2048]{1,0:T(8,128)(2,1)S(1)} %bitcast.10, bf16[64,2048]{1,0:T(8,128)(2,1)S(1)} %bitcast.15, bf16[64,2048]{1,0:T(8,128)(2,1)S(1)} %bitcast.16, f32[2,64]{1,0:T(2,128)S(1)} %pad_maximum_fusion.2.gain_ref, f32[4,16,128]{2,1,0:T(8,128)S(1)} %bitcast.12), custom_call_target="tpu_custom_call" | custom-call | flops 67108864 | bytes 1048576 | tf_op jit(solution)/shard_map/pallas_call | solution.py:214
  21.5 10.4 %all-to-all-start.1 = ((bf16[8,128,128]{2,1,0:T(8,128)(2,1)}), bf16[8,128,128]{2,1,0:T(8,128)(2,1)S(1)}, u32[]{:S(2)}, u32[]{:S(2)}) async-start(bf16[8,128,128]{2,1,0:T(8,128)(2,1)} %shard_map.75), calls=%async_computation.1 | async-start | bytes 524288 | tf_op jit(solution)/shard_map/all_to_all | solution.py:221
  31.9 0.4 shard_map.73
  32.3 2.6 %collective-permute-start = (bf16[256,128]{1,0:T(8,128)(2,1)S(1)}, bf16[256,128]{1,0:T(8,128)(2,1)S(1)}, u32[]{:S(2)}, u32[]{:S(2)}) collective-permute-start(bf16[256,128]{1,0:T(8,128)(2,1)S(1)} %shard_map.73), channel_id=1, source_target_pairs={{0,32},{32,0},{1,33},{33,1},{2,34},{34,2},{3,35},{35,3},{4,36},{36... | collective-permute-start | bytes 196616 | tf_op jit(solution)/shard_map/ppermute | solution.py:213
  35.0 8.2 %collective-permute-done = bf16[256,128]{1,0:T(8,128)(2,1)S(1)} collective-permute-done((bf16[256,128]{1,0:T(8,128)(2,1)S(1)}, bf16[256,128]{1,0:T(8,128)(2,1)S(1)}, u32[]{:S(2)}, u32[]{:S(2)}) %collective-permute-start) | collective-permute-done | bytes 65568 | tf_op jit(solution)/shard_map/ppermute | solution.py:213
  43.2 11.0 %all_gather.11.q_ref = bf16[8,256,128]{2,1,0:T(8,128)(2,1)S(1)} all-gather(bf16[2,256,128]{2,1,0:T(8,128)(2,1)S(1)} %pad_maximum_fusion), channel_id=1, replica_groups=mesh['zq'=8,'zp'=2,'y'=4,'x'=4,'c'=2] {'y'}, dimensions={0}, use_global_device_ids=true | all-gather | bytes 655360 | tf_op jit(solution)/shard_map/all_gather | solution.py:223
  54.2 0.1 shard_map.74.q_ref
  54.3 5.1 %shard_map.76 = bf16[16,144,128]{2,1,0:T(8,128)(2,1)S(1)} custom-call(bf16[4,4,64,256]{3,2,1,0:T(8,128)(2,1)S(1)} %shard_map.74.q_ref, bf16[8,128,128]{2,1,0:T(8,128)(2,1)S(1)} %all-to-all-done.1.kv_ref), custom_call_target="tpu_custom_call" | custom-call | flops 1073741824 | bytes 1048576 | tf_op jit(solution)/shard_map/pallas_call | solution.py:237
  59.4 0.0 copy-start
  59.4 19.6 %all_to_all.20.got_ref = bf16[16,144,128]{2,1,0:T(8,128)(2,1)S(1)} all-to-all(bf16[16,144,128]{2,1,0:T(8,128)(2,1)S(1)} %shard_map.76), channel_id=1, replica_groups=mesh['zq'=8,'zp'=2,'y'=4,'x'=4,'c'=2] {'y','zp','c'}, dimensions={0} | all-to-all | bytes 1179648 | tf_op jit(solution)/shard_map/all_to_all | solution.py:251
  79.1 0.6 shard_map.77
  79.6 8.7 %all_to_all.21 = bf16[4,16,2048]{2,1,0:T(8,128)(2,1)S(1)} all-to-all(bf16[4,16,2048]{2,1,0:T(8,128)(2,1)S(1)} %shard_map.77), channel_id=1, replica_groups=mesh['zq'=8,'zp'=2,'y'=4,'x'=4,'c'=2] {'x'}, dimensions={0} | all-to-all | bytes 524288 | tf_op jit(solution)/shard_map/all_to_all | solution.py:263
  88.4 0.7 reduce_sum.12
  (16 shorter events, 0.1 us)
Async XLA Ops:
  0.0 0.7 copy-start.5
  0.0 0.7 copy-start.6
  0.0 0.8 copy-start.4
  1.6 12.3 %all-to-all-start = ((bf16[4,16,2048]{2,1,0:T(8,128)(2,1)}), bf16[4,16,2048]{2,1,0:T(8,128)(2,1)S(1)}, u32[]{:S(2)}, u32[]{:S(2)}) async-start(bf16[4,16,2048]{2,1,0:T(8,128)(2,1)} %broadcast_in_dim.7), calls=%async_computation | async-start | bytes 524288 | tf_op jit(solution)/shard_map/all_to_all | solution.py:203
  6.4 13.9 %copy-start.2 = (bf16[2048,64]{0,1:T(8,128)(2,1)S(1)}, bf16[2048,64]{0,1:T(8,128)(2,1)}, u32[]{:S(2)}) copy-start(bf16[2048,64]{0,1:T(8,128)(2,1)} %param.9) | copy-start | bytes 786436
  6.4 13.9 %copy-start.3 = (bf16[2048,64]{0,1:T(8,128)(2,1)S(1)}, bf16[2048,64]{0,1:T(8,128)(2,1)}, u32[]{:S(2)}) copy-start(bf16[2048,64]{0,1:T(8,128)(2,1)} %param.10) | copy-start | bytes 786436
  6.4 47.9 %collective-permute-start.1 = (bf16[256,2048]{1,0:T(8,128)(2,1)}, bf16[256,2048]{1,0:T(8,128)(2,1)S(1)}, u32[]{:S(2)}, u32[]{:S(2)}) collective-permute-start(bf16[256,2048]{1,0:T(8,128)(2,1)} %own_ref.1), channel_id=1, source_target_pairs={{0,1},{1,0},{2,3},{3,2},{4,5},{5,4},{6,7},{7,6},{8,9},{9,8},{10,11... | collective-permute-start | bytes 3145736 | tf_op jit(solution)/shard_map/ppermute | solution.py:222
  20.3 11.6 %copy-start.1 = (bf16[2048,256]{1,0:T(8,128)(2,1)S(1)}, bf16[2048,256]{1,0:T(8,128)(2,1)}, u32[]{:S(2)}) copy-start(bf16[2048,256]{1,0:T(8,128)(2,1)} %w_ref.1) | copy-start | bytes 3145732
  21.5 32.8 %all-to-all-start.1 = ((bf16[8,128,128]{2,1,0:T(8,128)(2,1)}), bf16[8,128,128]{2,1,0:T(8,128)(2,1)S(1)}, u32[]{:S(2)}, u32[]{:S(2)}) async-start(bf16[8,128,128]{2,1,0:T(8,128)(2,1)} %shard_map.75), calls=%async_computation.1 | async-start | bytes 524288 | tf_op jit(solution)/shard_map/all_to_all | solution.py:221
  32.3 10.9 %collective-permute-start = (bf16[256,128]{1,0:T(8,128)(2,1)S(1)}, bf16[256,128]{1,0:T(8,128)(2,1)S(1)}, u32[]{:S(2)}, u32[]{:S(2)}) collective-permute-start(bf16[256,128]{1,0:T(8,128)(2,1)S(1)} %shard_map.73), channel_id=1, source_target_pairs={{0,32},{32,0},{1,33},{33,1},{2,34},{34,2},{3,35},{35,3},{4,36},{36... | collective-permute-start | bytes 196616 | tf_op jit(solution)/shard_map/ppermute | solution.py:213
  59.4 19.6 %copy-start = (bf16[256,2048]{1,0:T(8,128)(2,1)S(1)}, bf16[256,2048]{1,0:T(8,128)(2,1)}, u32[]{:S(2)}) copy-start(bf16[256,2048]{1,0:T(8,128)(2,1)} %own_ref.1) | copy-start | bytes 3145732

commit v6 on v5

--- a/solution.py
+++ b/solution.py
@@ -15,6 +15,7 @@
 TP = ("x", "c")
 ALL = SP + TP
 LOG2E = 1.4426950408889634
+X_LEAD, Y_LEAD, Z_LEAD = 2, 2, 5
 VMEM = pl.BlockSpec(memory_space=pltpu.VMEM)
 
 
@@ -41,6 +42,10 @@
         cosines += [ga * cos, gb * cos]
         sines += [-gb * sin, ga * sin]
     return jnp.concatenate(cosines, axis=0), jnp.concatenate(sines, axis=0)
+
+
+def led_by(lead, n):
+    return [[(lead + i) % n for i in range(n)]]
 
 
 def turned(u, cos, sin):
@@ -190,7 +195,7 @@
 
     n_x, n_c = lax.axis_size("x"), lax.axis_size("c")
     lane = jnp.arange(rows, dtype=jnp.int32)
-    core_of, x_of, row_of = lane // (n_x * mine), lane // mine % n_x, lane % mine
+    core_of, x_of, row_of = lane // (n_x * mine), (lane // mine + X_LEAD) % n_x, lane % mine
     position = lax.axis_index(SP) * rows + (x_of * n_c + core_of) * mine + row_of
     pairs = hd // 4
     freq = 10000.0 ** (-jnp.arange(pairs, dtype=F32) / pairs)
@@ -200,7 +205,7 @@
     gains = jnp.stack([q_gain, k_gain])
     tokens_in, tab, gains = lax.optimization_barrier((tokens_in, tab, gains))
     sent = jnp.broadcast_to(tokens_in[None], (lax.axis_size("x"), mine, d))
-    tokens = lax.all_to_all(sent, "x", 0, 0, tiled=True)
+    tokens = lax.all_to_all(sent, "x", 0, 0, tiled=True, axis_index_groups=led_by(X_LEAD, n_x))
     tokens = lax.all_gather(tokens, "c", axis=0).reshape(rows, d)
 
     query = call(
@@ -218,9 +223,11 @@
         2 * rows * d * 2 * hd,
         2 * d * (rows + 2 * hd),
     )(tokens, w_key.T, w_value.T, gains, tab)
-    kv = lax.all_to_all(kv, "zq", 0, 0, tiled=True)
+    kv = lax.all_to_all(kv, "zq", 0, 0, tiled=True, axis_index_groups=led_by(Z_LEAD, n_k))
     w_other = lax.ppermute(w_out, "c", [(0, 1), (1, 0)])
-    query = lax.all_gather(jnp.stack([query, other]), "y", axis=0, tiled=True)
+    query = lax.all_gather(
+        jnp.stack([query, other]), "y", axis=0, tiled=True, axis_index_groups=led_by(Y_LEAD, n_q // 2)
+    )
     query = pl.pallas_call(
         functools.partial(pair_kernel, hd),
         out_shape=jax.ShapeDtypeStruct((n_q // 2, heads, hd, 2 * rows), BF16),
@@ -248,7 +255,9 @@
             pltpu.VMEM((2, n_k * rows, 2 * rows), F32),
         ),
     )(query, kv)
-    got = lax.all_to_all(part, ("y", "zp", "c"), 0, 0, tiled=True)
+    got = lax.all_to_all(
+        part, ("y", "zp", "c"), 0, 0, tiled=True, axis_index_groups=led_by(Y_LEAD * 4, 2 * n_q)
+    )
 
     partial = pl.pallas_call(
         functools.partial(mix_kernel, hd),
@@ -260,7 +269,7 @@
             flops=2 * rows * qc * d, bytes_accessed=4 * d * qc, transcendentals=0
         ),
     )(core, got, w_out, w_other)
-    got = lax.all_to_all(partial, "x", 0, 0, tiled=True)
+    got = lax.all_to_all(partial, "x", 0, 0, tiled=True, axis_index_groups=led_by(X_LEAD, n_x))
     return got.astype(F32).sum(axis=0).astype(BF16)
 
 

time: 90.3 us -> 90.9 us (level)
  starting transfers between devices: 25.3 us -> 28.9 us
  blocking collectives: 45.7 us -> 42.5 us
  waiting for transfers between devices: 8.22 us -> 9.3 us
    all_to_all x2, starting transfers between devices: 15.2 us -> 19.5 us  [the longest x1 12.6 us: body(): lax.all_to_all(kv, 'zq', 0, 0, tiled=True, axis_index_groups=led_by(Z_LEA...]
    all_gather x1, blocking collectives: 6.35 us -> 3.46 us  [body(): tokens = lax.all_gather(tokens, 'c', axis=0).reshape(rows, d)]
    ppermute x1, waiting for transfers between devices: 8.21 us -> 9.3 us  [body(): other = lax.ppermute(query, 'zp', [(0, 1), (1, 0)])]
where the time goes in v6:
time: 90.9 us; the launch traced here: 90.4 us
  blocking collectives  42.5 us (47%)
  starting transfers between devices  28.9 us (32%)
  waiting for transfers between devices  9.3 us (10%)
  Pallas kernels  7.37 us (8%)
  local copies, waits for them, and re-layouts  1.38 us (2%)
    all_to_all x1, blocking collectives, body(): lax.all_to_all(part, ('y', 'zp', 'c'), 0, 0, tiled=True, axis_index_group...  20.1 us
    all_to_all x1, starting transfers between devices, body(): lax.all_to_all(kv, 'zq', 0, 0, tiled=True, axis_index_groups=led_by(Z_LEA...  12.6 us
    all_gather x1, blocking collectives, body(): lax.all_gather(jnp.stack([query, other]), 'y', axis=0, tiled=True, axis_i...  10.3 us
    ppermute x1, waiting for transfers between devices, body(): other = lax.ppermute(query, 'zp', [(0, 1), (1, 0)])  9.3 us
    all_to_all x1, blocking collectives, body(): lax.all_to_all(partial, 'x', 0, 0, tiled=True, axis_index_groups=led_by(X...  8.68 us
    all_to_all x1, starting transfers between devices, body(): lax.all_to_all(sent, 'x', 0, 0, tiled=True, axis_index_groups=led_by(X_LE...  6.94 us
    ppermute x1, starting transfers between devices, body(): w_other = lax.ppermute(w_out, 'c', [(0, 1), (1, 0)])  6.73 us
    pallas_call x1, Pallas kernels, body(): call(functools.partial(attend_kernel, hd), jax.ShapeDtypeStruct((2 * n_q,...  5.07 us
  transfers between devices with their start and end apart: 4, of which 1 were waited for; matrix products, arithmetic and copies ran while one was open for 0% of the time, Pallas kernels for 2%

profile of v6, /device:TPU:1, one launch (start us, length us, event | category | flops | bytes accessed | tf_op | source)
XLA Modules:
  0.0 90.4 jit_solution(16291033961045951003)
XLA Ops:
  0.0 0.0 copy-start.5
  0.0 0.0 copy-start.6
  0.0 0.0 copy-start.4
  0.1 0.6 copy-done.5
  0.7 0.0 copy-done.6
  0.7 0.1 multiply_cosine_fusion
  0.9 0.0 copy-done.4
  0.9 0.7 broadcast_in_dim.7
  1.6 6.9 %all-to-all-start = ((bf16[4,16,2048]{2,1,0:T(8,128)(2,1)}), bf16[4,16,2048]{2,1,0:T(8,128)(2,1)S(1)}, u32[]{:S(2)}, u32[]{:S(2)}) async-start(bf16[4,16,2048]{2,1,0:T(8,128)(2,1)} %broadcast_in_dim.7), calls=%async_computation | async-start | bytes 524288 | tf_op jit(solution)/shard_map/all_to_all | solution.py:208
  8.6 6.7 %collective-permute-start.1 = (bf16[256,2048]{1,0:T(8,128)(2,1)}, bf16[256,2048]{1,0:T(8,128)(2,1)S(1)}, u32[]{:S(2)}, u32[]{:S(2)}) collective-permute-start(bf16[256,2048]{1,0:T(8,128)(2,1)} %own_ref.1), channel_id=1, source_target_pairs={{0,1},{1,0},{2,3},{3,2},{4,5},{5,4},{6,7},{7,6},{8,9},{9,8},{10,11... | collective-permute-start | bytes 3145736 | tf_op jit(solution)/shard_map/ppermute | solution.py:227
  15.3 3.5 %all-gather = bf16[8,16,2048]{2,1,0:T(8,128)(2,1)S(1)} all-gather(bf16[4,16,2048]{2,1,0:T(8,128)(2,1)S(1)} %all-to-all-done), channel_id=2, replica_groups=mesh['zq'=8,'zp'=2,'y'=4,'x'=4,'c'=2] {'c'}, dimensions={0}, use_global_device_ids=true | all-gather | bytes 786432 | tf_op jit(solution)/shard_map/all_gather | solution.py:209
  18.8 1.2 %shard_map.75 = bf16[8,128,128]{2,1,0:T(8,128)(2,1)} custom-call(bf16[128,2048]{1,0:T(8,128)(2,1)S(1)} %bitcast.10, bf16[64,2048]{1,0:T(8,128)(2,1)S(1)} %bitcast.15, bf16[64,2048]{1,0:T(8,128)(2,1)S(1)} %bitcast.16, f32[2,64]{1,0:T(2,128)S(1)} %pad_maximum_fusion.2.gain_ref, f32[4,16,128]{2,1,0:T(8,128)S(1)} %bitcast.12), custom_call_target="tpu_custom_call" | custom-call | flops 67108864 | bytes 1048576 | tf_op jit(solution)/shard_map/pallas_call | solution.py:219
  20.0 12.6 %all-to-all-start.1 = ((bf16[8,128,128]{2,1,0:T(8,128)(2,1)}), bf16[8,128,128]{2,1,0:T(8,128)(2,1)S(1)}, u32[]{:S(2)}, u32[]{:S(2)}) async-start(bf16[8,128,128]{2,1,0:T(8,128)(2,1)} %shard_map.75), calls=%async_computation.1 | async-start | bytes 524288 | tf_op jit(solution)/shard_map/all_to_all | solution.py:226
  32.5 0.4 shard_map.73
  33.0 2.6 %collective-permute-start = (bf16[256,128]{1,0:T(8,128)(2,1)S(1)}, bf16[256,128]{1,0:T(8,128)(2,1)S(1)}, u32[]{:S(2)}, u32[]{:S(2)}) collective-permute-start(bf16[256,128]{1,0:T(8,128)(2,1)S(1)} %shard_map.73), channel_id=1, source_target_pairs={{0,32},{32,0},{1,33},{33,1},{2,34},{34,2},{3,35},{35,3},{4,36},{36... | collective-permute-start | bytes 196616 | tf_op jit(solution)/shard_map/ppermute | solution.py:218
  35.6 9.3 %collective-permute-done = bf16[256,128]{1,0:T(8,128)(2,1)S(1)} collective-permute-done((bf16[256,128]{1,0:T(8,128)(2,1)S(1)}, bf16[256,128]{1,0:T(8,128)(2,1)S(1)}, u32[]{:S(2)}, u32[]{:S(2)}) %collective-permute-start) | collective-permute-done | bytes 65568 | tf_op jit(solution)/shard_map/ppermute | solution.py:218
  44.9 10.3 %all_gather.11.q_ref = bf16[8,256,128]{2,1,0:T(8,128)(2,1)S(1)} all-gather(bf16[2,256,128]{2,1,0:T(8,128)(2,1)S(1)} %pad_maximum_fusion), channel_id=1, replica_groups={{16,24,0,8},{17,25,1,9},{18,26,2,10},{19,27,3,11},{20,28,4,12},{21,29,5..., dimensions={0}, use_global_device_ids=true | all-gather | bytes 655360 | tf_op jit(solution)/shard_map/all_gather | solution.py:228
  55.2 0.1 shard_map.74.q_ref
  55.3 5.1 %shard_map.76 = bf16[16,144,128]{2,1,0:T(8,128)(2,1)S(1)} custom-call(bf16[4,4,64,256]{3,2,1,0:T(8,128)(2,1)S(1)} %shard_map.74.q_ref, bf16[8,128,128]{2,1,0:T(8,128)(2,1)S(1)} %all-to-all-done.1.kv_ref), custom_call_target="tpu_custom_call" | custom-call | flops 1073741824 | bytes 1048576 | tf_op jit(solution)/shard_map/pallas_call | solution.py:244
  60.4 0.0 copy-start
  60.4 20.1 %all_to_all.20.got_ref = bf16[16,144,128]{2,1,0:T(8,128)(2,1)S(1)} all-to-all(bf16[16,144,128]{2,1,0:T(8,128)(2,1)S(1)} %shard_map.76), channel_id=1, replica_groups={{16,17,48,49,24,25,56,57,0,1,32,33,8,9,40,41},{18,19,50,51,26,27,58,59,..., dimensions={0} | all-to-all | bytes 1179648 | tf_op jit(solution)/shard_map/all_to_all | solution.py:258
  80.4 0.6 shard_map.77
  81.0 8.7 %all_to_all.21 = bf16[4,16,2048]{2,1,0:T(8,128)(2,1)S(1)} all-to-all(bf16[4,16,2048]{2,1,0:T(8,128)(2,1)S(1)} %shard_map.77), channel_id=1, replica_groups={{4,6,0,2},{5,7,1,3},{12,14,8,10},{13,15,9,11},{20,22,16,18},{21,23,17,1..., dimensions={0} | all-to-all | bytes 524288 | tf_op jit(solution)/shard_map/all_to_all | solution.py:272
  89.7 0.7 reduce_sum.12
  (16 shorter events, 0.1 us)
Async XLA Ops:
  0.0 0.7 copy-start.5
  0.0 0.7 copy-start.6
  0.0 0.8 copy-start.4
  1.6 13.7 %all-to-all-start = ((bf16[4,16,2048]{2,1,0:T(8,128)(2,1)}), bf16[4,16,2048]{2,1,0:T(8,128)(2,1)S(1)}, u32[]{:S(2)}, u32[]{:S(2)}) async-start(bf16[4,16,2048]{2,1,0:T(8,128)(2,1)} %broadcast_in_dim.7), calls=%async_computation | async-start | bytes 524288 | tf_op jit(solution)/shard_map/all_to_all | solution.py:208
  8.5 10.2 %copy-start.2 = (bf16[2048,64]{0,1:T(8,128)(2,1)S(1)}, bf16[2048,64]{0,1:T(8,128)(2,1)}, u32[]{:S(2)}) copy-start(bf16[2048,64]{0,1:T(8,128)(2,1)} %param.9) | copy-start | bytes 786436
  8.6 10.2 %copy-start.3 = (bf16[2048,64]{0,1:T(8,128)(2,1)S(1)}, bf16[2048,64]{0,1:T(8,128)(2,1)}, u32[]{:S(2)}) copy-start(bf16[2048,64]{0,1:T(8,128)(2,1)} %param.10) | copy-start | bytes 786436
  8.6 46.7 %collective-permute-start.1 = (bf16[256,2048]{1,0:T(8,128)(2,1)}, bf16[256,2048]{1,0:T(8,128)(2,1)S(1)}, u32[]{:S(2)}, u32[]{:S(2)}) collective-permute-start(bf16[256,2048]{1,0:T(8,128)(2,1)} %own_ref.1), channel_id=1, source_target_pairs={{0,1},{1,0},{2,3},{3,2},{4,5},{5,4},{6,7},{7,6},{8,9},{9,8},{10,11... | collective-permute-start | bytes 3145736 | tf_op jit(solution)/shard_map/ppermute | solution.py:227
  18.8 13.8 %copy-start.1 = (bf16[2048,256]{1,0:T(8,128)(2,1)S(1)}, bf16[2048,256]{1,0:T(8,128)(2,1)}, u32[]{:S(2)}) copy-start(bf16[2048,256]{1,0:T(8,128)(2,1)} %w_ref.1) | copy-start | bytes 3145732
  20.0 35.3 %all-to-all-start.1 = ((bf16[8,128,128]{2,1,0:T(8,128)(2,1)}), bf16[8,128,128]{2,1,0:T(8,128)(2,1)S(1)}, u32[]{:S(2)}, u32[]{:S(2)}) async-start(bf16[8,128,128]{2,1,0:T(8,128)(2,1)} %shard_map.75), calls=%async_computation.1 | async-start | bytes 524288 | tf_op jit(solution)/shard_map/all_to_all | solution.py:226
  33.0 12.0 %collective-permute-start = (bf16[256,128]{1,0:T(8,128)(2,1)S(1)}, bf16[256,128]{1,0:T(8,128)(2,1)S(1)}, u32[]{:S(2)}, u32[]{:S(2)}) collective-permute-start(bf16[256,128]{1,0:T(8,128)(2,1)S(1)} %shard_map.73), channel_id=1, source_target_pairs={{0,32},{32,0},{1,33},{33,1},{2,34},{34,2},{3,35},{35,3},{4,36},{36... | collective-permute-start | bytes 196616 | tf_op jit(solution)/shard_map/ppermute | solution.py:218
  60.4 20.1 %copy-start = (bf16[256,2048]{1,0:T(8,128)(2,1)S(1)}, bf16[256,2048]{1,0:T(8,128)(2,1)}, u32[]{:S(2)}) copy-start(bf16[256,2048]{1,0:T(8,128)(2,1)} %own_ref.1) | copy-start | bytes 3145732

commit v7 on v4

--- a/solution.py
+++ b/solution.py
@@ -15,6 +15,7 @@
 TP = ("x", "c")
 ALL = SP + TP
 LOG2E = 1.4426950408889634
+X_LEAD, Y_LEAD, Z_LEAD = 2, 2, 5
 VMEM = pl.BlockSpec(memory_space=pltpu.VMEM)
 
 
@@ -43,6 +44,10 @@
     return jnp.concatenate(cosines, axis=0), jnp.concatenate(sines, axis=0)
 
 
+def led_by(lead, n):
+    return [[(lead + i) % n for i in range(n)]]
+
+
 def turned(u, cos, sin):
     hd = u.shape[0]
     p = hd // 4
@@ -54,13 +59,8 @@
 NT = (((1,), (1,)), ((), ()))
 
 
-def in_order(x_ref):
-    n = x_ref.shape[0]
-    return jnp.concatenate([x_ref[(t % 2) * (n // 2) + t // 2] for t in range(n)], axis=0)
-
-
 def kv_kernel(copies, x_ref, wk_ref, wv_ref, gain_ref, tab_ref, out_ref):
-    x = in_order(x_ref)
+    x = x_ref[...]
     k = lax.dot_general(wk_ref[...], x, NT, preferred_element_type=F32)
     v = lax.dot_general(wv_ref[...], x, NT, preferred_element_type=F32)
     kt = turned(k.astype(BF16).astype(F32), *tables(gain_ref[1:2], tab_ref)).astype(BF16)
@@ -70,7 +70,7 @@
 
 
 def q_kernel(x_ref, w_ref, gain_ref, tab_ref, out_ref):
-    q = jnp.dot(in_order(x_ref), w_ref[...], preferred_element_type=F32)
+    q = jnp.dot(x_ref[...], w_ref[...], preferred_element_type=F32)
     qt = q.astype(BF16).astype(F32).T
     hd = gain_ref.shape[1]
     both = tables(gain_ref[0:1], tab_ref)
@@ -79,23 +79,12 @@
         out_ref[rows] = turned(qt[rows], *both).astype(BF16)
 
 
-def pair_kernel(hd, zp_ref, q_ref, out_ref):
+def attend_kernel(hd, zp_ref, q_ref, kv_ref, out_ref, k_ref, v_ref, s_ref):
     n_q, qc, rows = q_ref.shape
-    for i in range(n_q // 2):
-        for b in range(2):
-            block = 2 * i + (zp_ref[0] + b) % 2
-            for h in range(qc // hd):
-                out_ref[i, h, :, b * rows : (b + 1) * rows] = q_ref[
-                    block, h * hd : (h + 1) * hd, :
-                ]
-
-
-def attend_kernel(hd, q_ref, kv_ref, out_ref, k_ref, v_ref, s_ref):
-    n_pair, heads, _, rows = q_ref.shape
-    rows //= 2
+    n_pair, heads = n_q // 2, qc // hd
     n_k = kv_ref.shape[0]
     n_keys = n_k * rows
-    qc = heads * hd
+    spots = zp_ref[0], 1 - zp_ref[0]
     step = n_keys // 2
     scale = hd**-0.5 * LOG2E
     for j in range(n_k):
@@ -105,8 +94,11 @@
 
     def score(i, h, slot):
         top = None
+        q = jnp.concatenate(
+            [q_ref[2 * i + b, h * hd : (h + 1) * hd, :] for b in range(2)], axis=1
+        )
         for c in range(0, n_keys, step):
-            s = jnp.dot(k_ref[c : c + step, :], q_ref[i, h], preferred_element_type=F32)
+            s = jnp.dot(k_ref[c : c + step, :], q, preferred_element_type=F32)
             s_ref[slot, c : c + step] = s
             part = jnp.max(s.reshape(step // 8, 8, 2 * rows), axis=0)
             top = part if top is None else jnp.maximum(top, part)
@@ -126,7 +118,7 @@
             tops.append(top)
             sums.append(o[:1])
             for b in range(2):
-                out_ref[2 * i + b, h * hd : (h + 1) * hd, :] = o[
+                out_ref[2 * i + spots[b], h * hd : (h + 1) * hd, :] = o[
                     16:, b * rows : (b + 1) * rows
                 ].astype(BF16)
             top = later
@@ -134,7 +126,7 @@
         hi = total.astype(BF16).astype(F32)
         stats = jnp.concatenate(tops + [hi, total - hi, jnp.zeros_like(total)], axis=0).astype(BF16)
         for b in range(2):
-            out_ref[2 * i + b, qc:, :] = stats[:, b * rows : (b + 1) * rows]
+            out_ref[2 * i + spots[b], qc:, :] = stats[:, b * rows : (b + 1) * rows]
         return top
 
     lax.fori_loop(0, n_pair, pair, score(0, 0, 0))
@@ -160,7 +152,8 @@
     out = jnp.dot(mixed, w_ref[...], preferred_element_type=F32).astype(BF16)
     each = rows // n_tp
     for t in range(n_tp):
-        out_ref[t] = out[t * each : (t + 1) * each]
+        at = t % 2 * (n_tp // 2) + t // 2
+        out_ref[t] = out[at * each : (at + 1) * each]
 
 
 def body(tokens_in, w_query, w_key, w_value, w_out, q_gain, k_gain):
@@ -173,7 +166,10 @@
     n_q = lax.axis_size(("zp", "y"))
     heads = qc // hd
 
-    position = lax.axis_index(SP) * rows + jnp.arange(rows, dtype=jnp.int32)
+    n_x, n_c = lax.axis_size("x"), lax.axis_size("c")
+    lane = jnp.arange(rows, dtype=jnp.int32)
+    core_of, x_of, row_of = lane // (n_x * mine), (lane // mine + X_LEAD) % n_x, lane % mine
+    position = lax.axis_index(SP) * rows + (x_of * n_c + core_of) * mine + row_of
     pairs = hd // 4
     freq = 10000.0 ** (-jnp.arange(pairs, dtype=F32) / pairs)
     grid = jnp.stack([position // GRID_W, position % GRID_W]).astype(F32)
@@ -182,8 +178,8 @@
     gains = jnp.stack([q_gain, k_gain])
     tokens_in, tab, gains = lax.optimization_barrier((tokens_in, tab, gains))
     sent = jnp.broadcast_to(tokens_in[None], (lax.axis_size("x"), mine, d))
-    tokens = lax.all_to_all(sent, "x", 0, 0, tiled=True)
-    tokens = lax.all_gather(tokens, "c", axis=0).reshape(n_tp, mine, d)
+    tokens = lax.all_to_all(sent, "x", 0, 0, tiled=True, axis_index_groups=led_by(X_LEAD, n_x))
+    tokens = lax.all_gather(tokens, "c", axis=0).reshape(rows, d)
 
     query = call(
         q_kernel,
@@ -200,34 +196,30 @@
         2 * rows * d * 2 * hd,
         2 * d * (rows + 2 * hd),
     )(tokens, w_key.T, w_value.T, gains, tab)
-    kv = lax.all_to_all(kv, "zq", 0, 0, tiled=True)
-    query = lax.all_gather(jnp.stack([query, other]), "y", axis=0, tiled=True)
-    query = pl.pallas_call(
-        functools.partial(pair_kernel, hd),
-        out_shape=jax.ShapeDtypeStruct((n_q // 2, heads, hd, 2 * rows), BF16),
-        in_specs=[pl.BlockSpec(memory_space=pltpu.SMEM), VMEM],
+    kv = lax.all_to_all(kv, "zq", 0, 0, tiled=True, axis_index_groups=led_by(Z_LEAD, n_k))
+    query = lax.all_gather(
+        jnp.stack([query, other]), "y", axis=0, tiled=True, axis_index_groups=led_by(Y_LEAD, n_q // 2)
+    )
+    part = pl.pallas_call(
+        functools.partial(attend_kernel, hd),
+        out_shape=jax.ShapeDtypeStruct((n_q, qc + 16, rows), BF16),
+        in_specs=[pl.BlockSpec(memory_space=pltpu.SMEM), VMEM, VMEM],
         out_specs=VMEM,
-        compiler_params=pltpu.CompilerParams(vmem_limit_bytes=16 * 2**20),
-        cost_estimate=pl.CostEstimate(
-            flops=n_q * qc * rows, bytes_accessed=4 * n_q * qc * rows, transcendentals=0
-        ),
-    )(lax.axis_index("zp").astype(jnp.int32)[None], query)
-
-    part = call(
-        functools.partial(attend_kernel, hd),
-        jax.ShapeDtypeStruct((n_q, qc + 16, rows), BF16),
-        2,
-        4 * heads * n_q * rows * n_k * rows * hd,
-        4 * n_q * qc * rows,
-        exps=heads * n_q * rows * n_k * rows,
-        limit=32,
-        scratch=(
+        scratch_shapes=[
             pltpu.VMEM((n_k * rows, hd), BF16),
             pltpu.VMEM((hd + 16, n_k * rows), BF16),
             pltpu.VMEM((2, n_k * rows, 2 * rows), F32),
+        ],
+        compiler_params=pltpu.CompilerParams(vmem_limit_bytes=32 * 2**20),
+        cost_estimate=pl.CostEstimate(
+            flops=4 * heads * n_q * rows * n_k * rows * hd,
+            bytes_accessed=4 * n_q * qc * rows,
+            transcendentals=heads * n_q * rows * n_k * rows,
         ),
-    )(query, kv)
-    got = lax.all_to_all(part, ("y", "zp"), 0, 0, tiled=True)
+    )(lax.axis_index("zp").astype(jnp.int32)[None], query, kv)
+    got = lax.all_to_all(
+        part, ("y", "zp"), 0, 0, tiled=True, axis_index_groups=led_by(Y_LEAD * 2, n_q)
+    )
 
     partial = call(
         functools.partial(mix_kernel, hd, n_tp),
@@ -237,7 +229,9 @@
         2 * d * (rows + qc),
         scratch=(pltpu.VMEM((qc, rows), F32),),
     )(got, w_out)
-    got = lax.all_to_all(partial, TP, 0, 0, tiled=True)
+    got = lax.all_to_all(
+        partial, TP, 0, 0, tiled=True, axis_index_groups=led_by(X_LEAD * n_c, n_tp)
+    )
     return got.astype(F32).sum(axis=0).astype(BF16)
 
 

time: 89.6 us -> 89.6 us (level)
  blocking collectives: 58.1 us -> 57 us
  waiting for transfers between devices: 8.2 us -> 9.15 us
    ppermute x1, waiting for transfers between devices: 8.2 us -> 9.15 us  [body(): other = lax.ppermute(query, 'zp', [(0, 1), (1, 0)])]
    pallas_call x2 -> x1, Pallas kernels: 4.8 us -> 4.73 us  [body(): pl.pallas_call(functools.partial(attend_kernel, hd), out_shape=jax.ShapeD...]
  transfers between devices with their start and end apart: 2 -> 2, of which waited for: 1 -> 1; matrix products, arithmetic and copies ran while one was open for 0% -> 0% of each run, Pallas kernels for 1% -> 0%
where the time goes in v7:
time: 89.6 us; the launch traced here: 89.2 us
  blocking collectives  57 us (64%)
  starting transfers between devices  14.6 us (16%)
  waiting for transfers between devices  9.15 us (10%)
  Pallas kernels  6.8 us (8%)
  other arithmetic  0.92 us (1%)
    all_to_all x1, blocking collectives, body(): lax.all_to_all(partial, TP, 0, 0, tiled=True, axis_index_groups=led_by(X_...  16.5 us
    all_to_all x1, blocking collectives, body(): lax.all_to_all(part, ('y', 'zp'), 0, 0, tiled=True, axis_index_groups=led...  13.2 us
    all_to_all x1, starting transfers between devices, body(): lax.all_to_all(kv, 'zq', 0, 0, tiled=True, axis_index_groups=led_by(Z_LEA...  12 us
    all_gather x1, blocking collectives, body(): lax.all_gather(jnp.stack([query, other]), 'y', axis=0, tiled=True, axis_i...  10.4 us
    ppermute x1, waiting for transfers between devices, body(): other = lax.ppermute(query, 'zp', [(0, 1), (1, 0)])  9.15 us
    all_to_all x1, blocking collectives, body(): lax.all_to_all(sent, 'x', 0, 0, tiled=True, axis_index_groups=led_by(X_LE...  8.79 us
    all_gather x1, blocking collectives, body(): tokens = lax.all_gather(tokens, 'c', axis=0).reshape(rows, d)  8.08 us
    pallas_call x1, Pallas kernels, body(): pl.pallas_call(functools.partial(attend_kernel, hd), out_shape=jax.ShapeD...  4.73 us
  transfers between devices with their start and end apart: 2, of which 1 were waited for; matrix products, arithmetic and copies ran while one was open for 0% of the time, Pallas kernels for 0%

profile of v7, /device:TPU:1, one launch (start us, length us, event | category | flops | bytes accessed | tf_op | source)
XLA Modules:
  0.0 89.2 jit_solution(15475289635094058644)
XLA Ops:
  0.0 0.0 copy-start.5
  0.0 0.0 copy-start.6
  0.0 0.0 copy-start.4
  0.1 0.6 copy-done.5
  0.7 0.0 copy-done.6
  0.7 0.1 multiply_cosine_fusion
  0.9 0.0 copy-done.4
  0.9 8.8 %all_to_all.20 = bf16[4,16,2048]{2,1,0:T(8,128)(2,1)S(1)} all-to-all(bf16[4,16,2048]{2,1,0:T(8,128)(2,1)S(1)} %broadcast_in_dim.5), channel_id=1, replica_groups={{4,6,0,2},{5,7,1,3},{12,14,8,10},{13,15,9,11},{20,22,16,18},{21,23,17,1..., dimensions={0} | all-to-all | bytes 524288 | tf_op jit(solution)/shard_map/all_to_all | solution.py:181
  9.7 8.1 %all-gather = bf16[8,16,2048]{2,1,0:T(8,128)(2,1)S(1)} all-gather(bf16[4,16,2048]{2,1,0:T(8,128)(2,1)S(1)} %all_to_all.20), channel_id=2, replica_groups=mesh['zq'=8,'zp'=2,'y'=4,'x'=4,'c'=2] {'c'}, dimensions={0}, use_global_device_ids=true | all-gather | bytes 786432 | tf_op jit(solution)/shard_map/all_gather | solution.py:182
  17.8 0.0 copy-done.2
  17.8 1.2 %shard_map.74 = bf16[8,128,128]{2,1,0:T(8,128)(2,1)} custom-call(bf16[128,2048]{1,0:T(8,128)(2,1)S(1)} %bitcast.9, bf16[64,2048]{1,0:T(8,128)(2,1)S(1)} %bitcast.14, bf16[64,2048]{1,0:T(8,128)(2,1)S(1)} %bitcast.15, f32[2,64]{1,0:T(2,128)S(1)} %pad_maximum_fusion.2.gain_ref, f32[4,16,128]{2,1,0:T(8,128)S(1)} %bitcast.11), custom_call_target="tpu_custom_call" | custom-call | flops 67108864 | bytes 1048576 | tf_op jit(solution)/shard_map/pallas_call | solution.py:192
  19.0 12.0 %all-to-all-start.1 = ((bf16[8,128,128]{2,1,0:T(8,128)(2,1)}), bf16[8,128,128]{2,1,0:T(8,128)(2,1)S(1)}, u32[]{:S(2)}, u32[]{:S(2)}) async-start(bf16[8,128,128]{2,1,0:T(8,128)(2,1)} %shard_map.74), calls=%async_computation.1 | async-start | bytes 524288 | tf_op jit(solution)/shard_map/all_to_all | solution.py:199
  31.0 0.0 copy-done
  31.0 0.4 shard_map.73
  31.4 2.6 %collective-permute-start = (bf16[256,128]{1,0:T(8,128)(2,1)S(1)}, bf16[256,128]{1,0:T(8,128)(2,1)S(1)}, u32[]{:S(2)}, u32[]{:S(2)}) collective-permute-start(bf16[256,128]{1,0:T(8,128)(2,1)S(1)} %shard_map.73), channel_id=1, source_target_pairs={{0,32},{32,0},{1,33},{33,1},{2,34},{34,2},{3,35},{35,3},{4,36},{36... | collective-permute-start | bytes 196616 | tf_op jit(solution)/shard_map/ppermute | solution.py:191
  34.1 9.1 %collective-permute-done = bf16[256,128]{1,0:T(8,128)(2,1)S(1)} collective-permute-done((bf16[256,128]{1,0:T(8,128)(2,1)S(1)}, bf16[256,128]{1,0:T(8,128)(2,1)S(1)}, u32[]{:S(2)}, u32[]{:S(2)}) %collective-permute-start) | collective-permute-done | bytes 65568 | tf_op jit(solution)/shard_map/ppermute | solution.py:191
  43.2 10.4 %all_gather.11.q_ref = bf16[8,256,128]{2,1,0:T(8,128)(2,1)S(1)} all-gather(bf16[2,256,128]{2,1,0:T(8,128)(2,1)S(1)} %pad_maximum_fusion), channel_id=1, replica_groups={{16,24,0,8},{17,25,1,9},{18,26,2,10},{19,27,3,11},{20,28,4,12},{21,29,5..., dimensions={0}, use_global_device_ids=true | all-gather | bytes 655360 | tf_op jit(solution)/shard_map/all_gather | solution.py:200
  53.6 0.0 all-to-all-done.1.kv_ref
  53.6 4.7 %shard_map.75 = bf16[8,272,128]{2,1,0:T(8,128)(2,1)S(1)} custom-call(s32[1]{0:T(128)} %bitcast.zp_ref, bf16[8,256,128]{2,1,0:T(8,128)(2,1)S(1)} %all_gather.11.q_ref, bf16[8,128,128]{2,1,0:T(8,128)(2,1)S(1)} %all-to-all-done.1.kv_ref), custom_call_target="tpu_custom_call" | custom-call | flops 1073741824 | bytes 1048576 | tf_op jit(solution)/shard_map/pallas_call | solution.py:203
  58.4 0.0 copy-start.1
  58.4 13.2 %all_to_all.21.got_ref = bf16[8,272,128]{2,1,0:T(8,128)(2,1)S(1)} all-to-all(bf16[8,272,128]{2,1,0:T(8,128)(2,1)S(1)} %shard_map.75), channel_id=1, replica_groups={{16,48,24,56,0,32,8,40},{17,49,25,57,1,33,9,41},{18,50,26,58,2,34,10,42..., dimensions={0} | all-to-all | bytes 1114112 | tf_op jit(solution)/shard_map/all_to_all | solution.py:220
  71.6 0.4 shard_map.76
  72.0 16.5 %all_to_all.22 = bf16[8,16,2048]{2,1,0:T(8,128)(2,1)S(1)} all-to-all(bf16[8,16,2048]{2,1,0:T(8,128)(2,1)S(1)} %shard_map.76), channel_id=1, replica_groups={{4,5,6,7,0,1,2,3},{12,13,14,15,8,9,10,11},{20,21,22,23,16,17,18,19},{28..., dimensions={0} | all-to-all | bytes 1048576 | tf_op jit(solution)/shard_map/all_to_all | solution.py:232
  88.5 0.7 reduce_sum.12
  (12 shorter events, 0.1 us)
Async XLA Ops:
  0.0 0.7 copy-start.5
  0.0 0.7 copy-start.6
  0.0 0.8 copy-start.4
  9.7 8.1 %copy-start.2 = (bf16[2048,64]{0,1:T(8,128)(2,1)S(1)}, bf16[2048,64]{0,1:T(8,128)(2,1)}, u32[]{:S(2)}) copy-start(bf16[2048,64]{0,1:T(8,128)(2,1)} %param.9) | copy-start | bytes 786436
  9.7 8.1 %copy-start.3 = (bf16[2048,64]{0,1:T(8,128)(2,1)S(1)}, bf16[2048,64]{0,1:T(8,128)(2,1)}, u32[]{:S(2)}) copy-start(bf16[2048,64]{0,1:T(8,128)(2,1)} %param.10) | copy-start | bytes 786436
  17.8 13.2 %copy-start = (bf16[2048,256]{1,0:T(8,128)(2,1)S(1)}, bf16[2048,256]{1,0:T(8,128)(2,1)}, u32[]{:S(2)}) copy-start(bf16[2048,256]{1,0:T(8,128)(2,1)} %w_ref.2) | copy-start | bytes 3145732
  19.0 34.6 %all-to-all-start.1 = ((bf16[8,128,128]{2,1,0:T(8,128)(2,1)}), bf16[8,128,128]{2,1,0:T(8,128)(2,1)S(1)}, u32[]{:S(2)}, u32[]{:S(2)}) async-start(bf16[8,128,128]{2,1,0:T(8,128)(2,1)} %shard_map.74), calls=%async_computation.1 | async-start | bytes 524288 | tf_op jit(solution)/shard_map/all_to_all | solution.py:199
  31.4 11.8 %collective-permute-start = (bf16[256,128]{1,0:T(8,128)(2,1)S(1)}, bf16[256,128]{1,0:T(8,128)(2,1)S(1)}, u32[]{:S(2)}, u32[]{:S(2)}) collective-permute-start(bf16[256,128]{1,0:T(8,128)(2,1)S(1)} %shard_map.73), channel_id=1, source_target_pairs={{0,32},{32,0},{1,33},{33,1},{2,34},{34,2},{3,35},{35,3},{4,36},{36... | collective-permute-start | bytes 196616 | tf_op jit(solution)/shard_map/ppermute | solution.py:191
  58.4 13.2 %copy-start.1 = (bf16[256,2048]{1,0:T(8,128)(2,1)S(1)}, bf16[256,2048]{1,0:T(8,128)(2,1)}, u32[]{:S(2)}) copy-start(bf16[256,2048]{1,0:T(8,128)(2,1)} %w_ref.3) | copy-start | bytes 3145732

commit v8 on v7

--- a/solution.py
+++ b/solution.py
@@ -15,7 +15,7 @@
 TP = ("x", "c")
 ALL = SP + TP
 LOG2E = 1.4426950408889634
-X_LEAD, Y_LEAD, Z_LEAD = 2, 2, 5
+C_LEAD, OUT_LEAD, X_LEAD, Y_LEAD, Z_LEAD = 1, 5, 2, 2, 5
 VMEM = pl.BlockSpec(memory_space=pltpu.VMEM)
 
 
@@ -152,7 +152,8 @@
     out = jnp.dot(mixed, w_ref[...], preferred_element_type=F32).astype(BF16)
     each = rows // n_tp
     for t in range(n_tp):
-        at = t % 2 * (n_tp // 2) + t // 2
+        to = (OUT_LEAD + t) % n_tp
+        at = (to % 2 + C_LEAD) % 2 * (n_tp // 2) + (to // 2 - X_LEAD) % (n_tp // 2)
         out_ref[t] = out[at * each : (at + 1) * each]
 
 
@@ -168,7 +169,7 @@
 
     n_x, n_c = lax.axis_size("x"), lax.axis_size("c")
     lane = jnp.arange(rows, dtype=jnp.int32)
-    core_of, x_of, row_of = lane // (n_x * mine), (lane // mine + X_LEAD) % n_x, lane % mine
+    core_of, x_of, row_of = (lane // (n_x * mine) + C_LEAD) % n_c, (lane // mine + X_LEAD) % n_x, lane % mine
     position = lax.axis_index(SP) * rows + (x_of * n_c + core_of) * mine + row_of
     pairs = hd // 4
     freq = 10000.0 ** (-jnp.arange(pairs, dtype=F32) / pairs)
@@ -179,7 +180,7 @@
     tokens_in, tab, gains = lax.optimization_barrier((tokens_in, tab, gains))
     sent = jnp.broadcast_to(tokens_in[None], (lax.axis_size("x"), mine, d))
     tokens = lax.all_to_all(sent, "x", 0, 0, tiled=True, axis_index_groups=led_by(X_LEAD, n_x))
-    tokens = lax.all_gather(tokens, "c", axis=0).reshape(rows, d)
+    tokens = lax.all_gather(tokens, "c", axis=0, axis_index_groups=led_by(C_LEAD, n_c)).reshape(rows, d)
 
     query = call(
         q_kernel,
@@ -230,7 +231,7 @@
         scratch=(pltpu.VMEM((qc, rows), F32),),
     )(got, w_out)
     got = lax.all_to_all(
-        partial, TP, 0, 0, tiled=True, axis_index_groups=led_by(X_LEAD * n_c, n_tp)
+        partial, TP, 0, 0, tiled=True, axis_index_groups=led_by(OUT_LEAD, n_tp)
     )
     return got.astype(F32).sum(axis=0).astype(BF16)
 

time: 89.6 us -> 88.4 us (0.987)
  blocking collectives: 57 us -> 55.7 us
    all_to_all x1, blocking collectives: 16.5 us -> 15.2 us  [body(): lax.all_to_all(partial, TP, 0, 0, tiled=True, axis_index_groups=led_by(OU...]
where the time goes in v8:
time: 88.4 us; the launch traced here: 88 us
  blocking collectives  55.7 us (63%)
  starting transfers between devices  14.6 us (17%)
  waiting for transfers between devices  9.15 us (10%)
  Pallas kernels  6.8 us (8%)
  other arithmetic  0.92 us (1%)
    all_to_all x1, blocking collectives, body(): lax.all_to_all(partial, TP, 0, 0, tiled=True, axis_index_groups=led_by(OU...  15.2 us
    all_to_all x1, blocking collectives, body(): lax.all_to_all(part, ('y', 'zp'), 0, 0, tiled=True, axis_index_groups=led...  13.2 us
    all_to_all x1, starting transfers between devices, body(): lax.all_to_all(kv, 'zq', 0, 0, tiled=True, axis_index_groups=led_by(Z_LEA...  12 us
    all_gather x1, blocking collectives, body(): lax.all_gather(jnp.stack([query, other]), 'y', axis=0, tiled=True, axis_i...  10.4 us
    ppermute x1, waiting for transfers between devices, body(): other = lax.ppermute(query, 'zp', [(0, 1), (1, 0)])  9.15 us
    all_to_all x1, blocking collectives, body(): lax.all_to_all(sent, 'x', 0, 0, tiled=True, axis_index_groups=led_by(X_LE...  8.79 us
    all_gather x1, blocking collectives, body(): lax.all_gather(tokens, 'c', axis=0, axis_index_groups=led_by(C_LEAD, n_c))  8.08 us
    pallas_call x1, Pallas kernels, body(): pl.pallas_call(functools.partial(attend_kernel, hd), out_shape=jax.ShapeD...  4.73 us
  transfers between devices with their start and end apart: 2, of which 1 were waited for; matrix products, arithmetic and copies ran while one was open for 0% of the time, Pallas kernels for 0%

profile of v8, /device:TPU:1, one launch (start us, length us, event | category | flops | bytes accessed | tf_op | source)
XLA Modules:
  0.0 88.0 jit_solution(8025802074724625980)
XLA Ops:
  0.0 0.0 copy-start.5
  0.0 0.0 copy-start.6
  0.0 0.0 copy-start.4
  0.1 0.6 copy-done.5
  0.7 0.0 copy-done.6
  0.7 0.1 multiply_cosine_fusion
  0.9 0.0 copy-done.4
  0.9 8.8 %all_to_all.20 = bf16[4,16,2048]{2,1,0:T(8,128)(2,1)S(1)} all-to-all(bf16[4,16,2048]{2,1,0:T(8,128)(2,1)S(1)} %broadcast_in_dim.5), channel_id=1, replica_groups={{4,6,0,2},{5,7,1,3},{12,14,8,10},{13,15,9,11},{20,22,16,18},{21,23,17,1..., dimensions={0} | all-to-all | bytes 524288 | tf_op jit(solution)/shard_map/all_to_all | solution.py:182
  9.7 8.1 %all-gather = bf16[8,16,2048]{2,1,0:T(8,128)(2,1)S(1)} all-gather(bf16[4,16,2048]{2,1,0:T(8,128)(2,1)S(1)} %all_to_all.20), channel_id=2, replica_groups={{1,0},{3,2},{5,4},{7,6},{9,8},{11,10},{13,12},{15,14},{17,16},{19,18},{..., dimensions={0}, use_global_device_ids=true | all-gather | bytes 786432 | tf_op jit(solution)/shard_map/all_gather | solution.py:183
  17.8 0.0 copy-done.2
  17.8 1.2 %shard_map.74 = bf16[8,128,128]{2,1,0:T(8,128)(2,1)} custom-call(bf16[128,2048]{1,0:T(8,128)(2,1)S(1)} %bitcast.9, bf16[64,2048]{1,0:T(8,128)(2,1)S(1)} %bitcast.14, bf16[64,2048]{1,0:T(8,128)(2,1)S(1)} %bitcast.15, f32[2,64]{1,0:T(2,128)S(1)} %pad_maximum_fusion.2.gain_ref, f32[4,16,128]{2,1,0:T(8,128)S(1)} %bitcast.11), custom_call_target="tpu_custom_call" | custom-call | flops 67108864 | bytes 1048576 | tf_op jit(solution)/shard_map/pallas_call | solution.py:193
  19.0 12.0 %all-to-all-start.1 = ((bf16[8,128,128]{2,1,0:T(8,128)(2,1)}), bf16[8,128,128]{2,1,0:T(8,128)(2,1)S(1)}, u32[]{:S(2)}, u32[]{:S(2)}) async-start(bf16[8,128,128]{2,1,0:T(8,128)(2,1)} %shard_map.74), calls=%async_computation.1 | async-start | bytes 524288 | tf_op jit(solution)/shard_map/all_to_all | solution.py:200
  31.0 0.0 copy-done
  31.0 0.4 shard_map.73
  31.4 2.6 %collective-permute-start = (bf16[256,128]{1,0:T(8,128)(2,1)S(1)}, bf16[256,128]{1,0:T(8,128)(2,1)S(1)}, u32[]{:S(2)}, u32[]{:S(2)}) collective-permute-start(bf16[256,128]{1,0:T(8,128)(2,1)S(1)} %shard_map.73), channel_id=1, source_target_pairs={{0,32},{32,0},{1,33},{33,1},{2,34},{34,2},{3,35},{35,3},{4,36},{36... | collective-permute-start | bytes 196616 | tf_op jit(solution)/shard_map/ppermute | solution.py:192
  34.1 9.1 %collective-permute-done = bf16[256,128]{1,0:T(8,128)(2,1)S(1)} collective-permute-done((bf16[256,128]{1,0:T(8,128)(2,1)S(1)}, bf16[256,128]{1,0:T(8,128)(2,1)S(1)}, u32[]{:S(2)}, u32[]{:S(2)}) %collective-permute-start) | collective-permute-done | bytes 65568 | tf_op jit(solution)/shard_map/ppermute | solution.py:192
  43.2 10.4 %all_gather.11.q_ref = bf16[8,256,128]{2,1,0:T(8,128)(2,1)S(1)} all-gather(bf16[2,256,128]{2,1,0:T(8,128)(2,1)S(1)} %pad_maximum_fusion), channel_id=1, replica_groups={{16,24,0,8},{17,25,1,9},{18,26,2,10},{19,27,3,11},{20,28,4,12},{21,29,5..., dimensions={0}, use_global_device_ids=true | all-gather | bytes 655360 | tf_op jit(solution)/shard_map/all_gather | solution.py:201
  53.6 0.0 all-to-all-done.1.kv_ref
  53.6 4.7 %shard_map.75 = bf16[8,272,128]{2,1,0:T(8,128)(2,1)S(1)} custom-call(s32[1]{0:T(128)} %bitcast.zp_ref, bf16[8,256,128]{2,1,0:T(8,128)(2,1)S(1)} %all_gather.11.q_ref, bf16[8,128,128]{2,1,0:T(8,128)(2,1)S(1)} %all-to-all-done.1.kv_ref), custom_call_target="tpu_custom_call" | custom-call | flops 1073741824 | bytes 1048576 | tf_op jit(solution)/shard_map/pallas_call | solution.py:204
  58.4 0.0 copy-start.1
  58.4 13.2 %all_to_all.21.got_ref = bf16[8,272,128]{2,1,0:T(8,128)(2,1)S(1)} all-to-all(bf16[8,272,128]{2,1,0:T(8,128)(2,1)S(1)} %shard_map.75), channel_id=1, replica_groups={{16,48,24,56,0,32,8,40},{17,49,25,57,1,33,9,41},{18,50,26,58,2,34,10,42..., dimensions={0} | all-to-all | bytes 1114112 | tf_op jit(solution)/shard_map/all_to_all | solution.py:221
  71.6 0.4 shard_map.76
  72.0 15.2 %all_to_all.22 = bf16[8,16,2048]{2,1,0:T(8,128)(2,1)S(1)} all-to-all(bf16[8,16,2048]{2,1,0:T(8,128)(2,1)S(1)} %shard_map.76), channel_id=1, replica_groups={{5,6,7,0,1,2,3,4},{13,14,15,8,9,10,11,12},{21,22,23,16,17,18,19,20},{29..., dimensions={0} | all-to-all | bytes 1048576 | tf_op jit(solution)/shard_map/all_to_all | solution.py:233
  87.3 0.7 reduce_sum.12
  (12 shorter events, 0.1 us)
Async XLA Ops:
  0.0 0.7 copy-start.5
  0.0 0.7 copy-start.6
  0.0 0.8 copy-start.4
  9.7 8.1 %copy-start.2 = (bf16[2048,64]{0,1:T(8,128)(2,1)S(1)}, bf16[2048,64]{0,1:T(8,128)(2,1)}, u32[]{:S(2)}) copy-start(bf16[2048,64]{0,1:T(8,128)(2,1)} %param.9) | copy-start | bytes 786436
  9.7 8.1 %copy-start.3 = (bf16[2048,64]{0,1:T(8,128)(2,1)S(1)}, bf16[2048,64]{0,1:T(8,128)(2,1)}, u32[]{:S(2)}) copy-start(bf16[2048,64]{0,1:T(8,128)(2,1)} %param.10) | copy-start | bytes 786436
  17.8 13.2 %copy-start = (bf16[2048,256]{1,0:T(8,128)(2,1)S(1)}, bf16[2048,256]{1,0:T(8,128)(2,1)}, u32[]{:S(2)}) copy-start(bf16[2048,256]{1,0:T(8,128)(2,1)} %w_ref.2) | copy-start | bytes 3145732
  19.0 34.6 %all-to-all-start.1 = ((bf16[8,128,128]{2,1,0:T(8,128)(2,1)}), bf16[8,128,128]{2,1,0:T(8,128)(2,1)S(1)}, u32[]{:S(2)}, u32[]{:S(2)}) async-start(bf16[8,128,128]{2,1,0:T(8,128)(2,1)} %shard_map.74), calls=%async_computation.1 | async-start | bytes 524288 | tf_op jit(solution)/shard_map/all_to_all | solution.py:200
  31.4 11.8 %collective-permute-start = (bf16[256,128]{1,0:T(8,128)(2,1)S(1)}, bf16[256,128]{1,0:T(8,128)(2,1)S(1)}, u32[]{:S(2)}, u32[]{:S(2)}) collective-permute-start(bf16[256,128]{1,0:T(8,128)(2,1)S(1)} %shard_map.73), channel_id=1, source_target_pairs={{0,32},{32,0},{1,33},{33,1},{2,34},{34,2},{3,35},{35,3},{4,36},{36... | collective-permute-start | bytes 196616 | tf_op jit(solution)/shard_map/ppermute | solution.py:192
  58.4 13.2 %copy-start.1 = (bf16[256,2048]{1,0:T(8,128)(2,1)S(1)}, bf16[256,2048]{1,0:T(8,128)(2,1)}, u32[]{:S(2)}) copy-start(bf16[256,2048]{1,0:T(8,128)(2,1)} %w_ref.3) | copy-start | bytes 3145732

commit v9 on v8

--- a/solution.py
+++ b/solution.py
@@ -15,7 +15,8 @@
 TP = ("x", "c")
 ALL = SP + TP
 LOG2E = 1.4426950408889634
-C_LEAD, OUT_LEAD, X_LEAD, Y_LEAD, Z_LEAD = 1, 5, 2, 2, 5
+C_LEAD, OUT_LEAD, X_LEAD, Z_LEAD = 1, 5, 2, 5
+Y_ORDER = 2, 1, 0, 3
 VMEM = pl.BlockSpec(memory_space=pltpu.VMEM)
 
 
@@ -153,7 +154,7 @@
     each = rows // n_tp
     for t in range(n_tp):
         to = (OUT_LEAD + t) % n_tp
-        at = (to % 2 + C_LEAD) % 2 * (n_tp // 2) + (to // 2 - X_LEAD) % (n_tp // 2)
+        at = (to % 2 + C_LEAD) % 2 * (n_tp // 2) + (X_LEAD - to // 2) % (n_tp // 2)
         out_ref[t] = out[at * each : (at + 1) * each]
 
 
@@ -169,7 +170,7 @@
 
     n_x, n_c = lax.axis_size("x"), lax.axis_size("c")
     lane = jnp.arange(rows, dtype=jnp.int32)
-    core_of, x_of, row_of = (lane // (n_x * mine) + C_LEAD) % n_c, (lane // mine + X_LEAD) % n_x, lane % mine
+    core_of, x_of, row_of = (lane // (n_x * mine) + C_LEAD) % n_c, (X_LEAD - lane // mine) % n_x, lane % mine
     position = lax.axis_index(SP) * rows + (x_of * n_c + core_of) * mine + row_of
     pairs = hd // 4
     freq = 10000.0 ** (-jnp.arange(pairs, dtype=F32) / pairs)
@@ -179,7 +180,7 @@
     gains = jnp.stack([q_gain, k_gain])
     tokens_in, tab, gains = lax.optimization_barrier((tokens_in, tab, gains))
     sent = jnp.broadcast_to(tokens_in[None], (lax.axis_size("x"), mine, d))
-    tokens = lax.all_to_all(sent, "x", 0, 0, tiled=True, axis_index_groups=led_by(X_LEAD, n_x))
+    tokens = lax.all_to_all(sent, "x", 0, 0, tiled=True, axis_index_groups=[[(X_LEAD - i) % n_x for i in range(n_x)]])
     tokens = lax.all_gather(tokens, "c", axis=0, axis_index_groups=led_by(C_LEAD, n_c)).reshape(rows, d)
 
     query = call(
@@ -199,7 +200,7 @@
     )(tokens, w_key.T, w_value.T, gains, tab)
     kv = lax.all_to_all(kv, "zq", 0, 0, tiled=True, axis_index_groups=led_by(Z_LEAD, n_k))
     query = lax.all_gather(
-        jnp.stack([query, other]), "y", axis=0, tiled=True, axis_index_groups=led_by(Y_LEAD, n_q // 2)
+        jnp.stack([query, other]), "y", axis=0, tiled=True, axis_index_groups=[list(Y_ORDER)]
     )
     part = pl.pallas_call(
         functools.partial(attend_kernel, hd),
@@ -219,7 +220,7 @@
         ),
     )(lax.axis_index("zp").astype(jnp.int32)[None], query, kv)
     got = lax.all_to_all(
-        part, ("y", "zp"), 0, 0, tiled=True, axis_index_groups=led_by(Y_LEAD * 2, n_q)
+        part, ("y", "zp"), 0, 0, tiled=True, axis_index_groups=[[2 * y + p for y in Y_ORDER for p in range(2)]]
     )
 
     partial = call(

time: 88.4 us -> 88.3 us (level)
  no operation moved by 1% of the time
where the time goes in v9:
time: 88.3 us; the launch traced here: 87.9 us
  blocking collectives  55.6 us (63%)
  starting transfers between devices  14.6 us (17%)
  waiting for transfers between devices  9.15 us (10%)
  Pallas kernels  6.8 us (8%)
  other arithmetic  0.92 us (1%)
    all_to_all x1, blocking collectives, body(): lax.all_to_all(partial, TP, 0, 0, tiled=True, axis_index_groups=led_by(OU...  15.1 us
    all_to_all x1, blocking collectives, body(): lax.all_to_all(part, ('y', 'zp'), 0, 0, tiled=True, axis_index_groups=[[2...  13.3 us
    all_to_all x1, starting transfers between devices, body(): lax.all_to_all(kv, 'zq', 0, 0, tiled=True, axis_index_groups=led_by(Z_LEA...  12 us
    all_gather x1, blocking collectives, body(): lax.all_gather(jnp.stack([query, other]), 'y', axis=0, tiled=True, axis_i...  10.4 us
    ppermute x1, waiting for transfers between devices, body(): other = lax.ppermute(query, 'zp', [(0, 1), (1, 0)])  9.15 us
    all_to_all x1, blocking collectives, body(): lax.all_to_all(sent, 'x', 0, 0, tiled=True, axis_index_groups=[[(X_LEAD -...  8.79 us
    all_gather x1, blocking collectives, body(): lax.all_gather(tokens, 'c', axis=0, axis_index_groups=led_by(C_LEAD, n_c))  8.07 us
    pallas_call x1, Pallas kernels, body(): pl.pallas_call(functools.partial(attend_kernel, hd), out_shape=jax.ShapeD...  4.73 us
  transfers between devices with their start and end apart: 2, of which 1 were waited for; matrix products, arithmetic and copies ran while one was open for 0% of the time, Pallas kernels for 0%

profile of v9, /device:TPU:1, one launch (start us, length us, event | category | flops | bytes accessed | tf_op | source)
XLA Modules:
  0.0 87.9 jit_solution(9457865778239448288)
XLA Ops:
  0.0 0.0 copy-start.5
  0.0 0.0 copy-start.6
  0.0 0.0 copy-start.4
  0.1 0.6 copy-done.5
  0.7 0.0 copy-done.6
  0.7 0.1 multiply_cosine_fusion
  0.9 0.0 copy-done.4
  0.9 8.8 %all_to_all.20 = bf16[4,16,2048]{2,1,0:T(8,128)(2,1)S(1)} all-to-all(bf16[4,16,2048]{2,1,0:T(8,128)(2,1)S(1)} %broadcast_in_dim.5), channel_id=1, replica_groups={{4,2,0,6},{5,3,1,7},{12,10,8,14},{13,11,9,15},{20,18,16,22},{21,19,17,2..., dimensions={0} | all-to-all | bytes 524288 | tf_op jit(solution)/shard_map/all_to_all | solution.py:183
  9.7 8.1 %all-gather = bf16[8,16,2048]{2,1,0:T(8,128)(2,1)S(1)} all-gather(bf16[4,16,2048]{2,1,0:T(8,128)(2,1)S(1)} %all_to_all.20), channel_id=2, replica_groups={{1,0},{3,2},{5,4},{7,6},{9,8},{11,10},{13,12},{15,14},{17,16},{19,18},{..., dimensions={0}, use_global_device_ids=true | all-gather | bytes 786432 | tf_op jit(solution)/shard_map/all_gather | solution.py:184
  17.8 0.0 copy-done.2
  17.8 1.2 %shard_map.74 = bf16[8,128,128]{2,1,0:T(8,128)(2,1)} custom-call(bf16[128,2048]{1,0:T(8,128)(2,1)S(1)} %bitcast.9, bf16[64,2048]{1,0:T(8,128)(2,1)S(1)} %bitcast.14, bf16[64,2048]{1,0:T(8,128)(2,1)S(1)} %bitcast.15, f32[2,64]{1,0:T(2,128)S(1)} %pad_maximum_fusion.2.gain_ref, f32[4,16,128]{2,1,0:T(8,128)S(1)} %bitcast.11), custom_call_target="tpu_custom_call" | custom-call | flops 67108864 | bytes 1048576 | tf_op jit(solution)/shard_map/pallas_call | solution.py:194
  19.0 12.0 %all-to-all-start.1 = ((bf16[8,128,128]{2,1,0:T(8,128)(2,1)}), bf16[8,128,128]{2,1,0:T(8,128)(2,1)S(1)}, u32[]{:S(2)}, u32[]{:S(2)}) async-start(bf16[8,128,128]{2,1,0:T(8,128)(2,1)} %shard_map.74), calls=%async_computation.1 | async-start | bytes 524288 | tf_op jit(solution)/shard_map/all_to_all | solution.py:201
  31.0 0.0 copy-done
  31.0 0.4 shard_map.73
  31.4 2.6 %collective-permute-start = (bf16[256,128]{1,0:T(8,128)(2,1)S(1)}, bf16[256,128]{1,0:T(8,128)(2,1)S(1)}, u32[]{:S(2)}, u32[]{:S(2)}) collective-permute-start(bf16[256,128]{1,0:T(8,128)(2,1)S(1)} %shard_map.73), channel_id=1, source_target_pairs={{0,32},{32,0},{1,33},{33,1},{2,34},{34,2},{3,35},{35,3},{4,36},{36... | collective-permute-start | bytes 196616 | tf_op jit(solution)/shard_map/ppermute | solution.py:193
  34.1 9.1 %collective-permute-done = bf16[256,128]{1,0:T(8,128)(2,1)S(1)} collective-permute-done((bf16[256,128]{1,0:T(8,128)(2,1)S(1)}, bf16[256,128]{1,0:T(8,128)(2,1)S(1)}, u32[]{:S(2)}, u32[]{:S(2)}) %collective-permute-start) | collective-permute-done | bytes 65568 | tf_op jit(solution)/shard_map/ppermute | solution.py:193
  43.2 10.4 %all_gather.11.q_ref = bf16[8,256,128]{2,1,0:T(8,128)(2,1)S(1)} all-gather(bf16[2,256,128]{2,1,0:T(8,128)(2,1)S(1)} %pad_maximum_fusion), channel_id=1, replica_groups={{16,8,0,24},{17,9,1,25},{18,10,2,26},{19,11,3,27},{20,12,4,28},{21,13,5..., dimensions={0}, use_global_device_ids=true | all-gather | bytes 655360 | tf_op jit(solution)/shard_map/all_gather | solution.py:202
  53.6 0.0 all-to-all-done.1.kv_ref
  53.6 4.7 %shard_map.75 = bf16[8,272,128]{2,1,0:T(8,128)(2,1)S(1)} custom-call(s32[1]{0:T(128)} %bitcast.zp_ref, bf16[8,256,128]{2,1,0:T(8,128)(2,1)S(1)} %all_gather.11.q_ref, bf16[8,128,128]{2,1,0:T(8,128)(2,1)S(1)} %all-to-all-done.1.kv_ref), custom_call_target="tpu_custom_call" | custom-call | flops 1073741824 | bytes 1048576 | tf_op jit(solution)/shard_map/pallas_call | solution.py:205
  58.4 0.0 copy-start.1
  58.4 13.3 %all_to_all.21.got_ref = bf16[8,272,128]{2,1,0:T(8,128)(2,1)S(1)} all-to-all(bf16[8,272,128]{2,1,0:T(8,128)(2,1)S(1)} %shard_map.75), channel_id=1, replica_groups={{16,48,8,40,0,32,24,56},{17,49,9,41,1,33,25,57},{18,50,10,42,2,34,26,58..., dimensions={0} | all-to-all | bytes 1114112 | tf_op jit(solution)/shard_map/all_to_all | solution.py:222
  71.7 0.4 shard_map.76
  72.1 15.1 %all_to_all.22 = bf16[8,16,2048]{2,1,0:T(8,128)(2,1)S(1)} all-to-all(bf16[8,16,2048]{2,1,0:T(8,128)(2,1)S(1)} %shard_map.76), channel_id=1, replica_groups={{5,6,7,0,1,2,3,4},{13,14,15,8,9,10,11,12},{21,22,23,16,17,18,19,20},{29..., dimensions={0} | all-to-all | bytes 1048576 | tf_op jit(solution)/shard_map/all_to_all | solution.py:234
  87.2 0.7 reduce_sum.12
  (12 shorter events, 0.1 us)
Async XLA Ops:
  0.0 0.7 copy-start.5
  0.0 0.7 copy-start.6
  0.0 0.8 copy-start.4
  9.7 8.1 %copy-start.2 = (bf16[2048,64]{0,1:T(8,128)(2,1)S(1)}, bf16[2048,64]{0,1:T(8,128)(2,1)}, u32[]{:S(2)}) copy-start(bf16[2048,64]{0,1:T(8,128)(2,1)} %param.9) | copy-start | bytes 786436
  9.7 8.1 %copy-start.3 = (bf16[2048,64]{0,1:T(8,128)(2,1)S(1)}, bf16[2048,64]{0,1:T(8,128)(2,1)}, u32[]{:S(2)}) copy-start(bf16[2048,64]{0,1:T(8,128)(2,1)} %param.10) | copy-start | bytes 786436
  17.8 13.2 %copy-start = (bf16[2048,256]{1,0:T(8,128)(2,1)S(1)}, bf16[2048,256]{1,0:T(8,128)(2,1)}, u32[]{:S(2)}) copy-start(bf16[2048,256]{1,0:T(8,128)(2,1)} %w_ref.2) | copy-start | bytes 3145732
  19.0 34.6 %all-to-all-start.1 = ((bf16[8,128,128]{2,1,0:T(8,128)(2,1)}), bf16[8,128,128]{2,1,0:T(8,128)(2,1)S(1)}, u32[]{:S(2)}, u32[]{:S(2)}) async-start(bf16[8,128,128]{2,1,0:T(8,128)(2,1)} %shard_map.74), calls=%async_computation.1 | async-start | bytes 524288 | tf_op jit(solution)/shard_map/all_to_all | solution.py:201
  31.4 11.8 %collective-permute-start = (bf16[256,128]{1,0:T(8,128)(2,1)S(1)}, bf16[256,128]{1,0:T(8,128)(2,1)S(1)}, u32[]{:S(2)}, u32[]{:S(2)}) collective-permute-start(bf16[256,128]{1,0:T(8,128)(2,1)S(1)} %shard_map.73), channel_id=1, source_target_pairs={{0,32},{32,0},{1,33},{33,1},{2,34},{34,2},{3,35},{35,3},{4,36},{36... | collective-permute-start | bytes 196616 | tf_op jit(solution)/shard_map/ppermute | solution.py:193
  58.4 13.3 %copy-start.1 = (bf16[256,2048]{1,0:T(8,128)(2,1)S(1)}, bf16[256,2048]{1,0:T(8,128)(2,1)}, u32[]{:S(2)}) copy-start(bf16[256,2048]{1,0:T(8,128)(2,1)} %w_ref.3) | copy-start | bytes 3145732

commit v10 on v9

--- a/solution.py
+++ b/solution.py
@@ -119,7 +119,7 @@
             tops.append(top)
             sums.append(o[:1])
             for b in range(2):
-                out_ref[2 * i + spots[b], h * hd : (h + 1) * hd, :] = o[
+                out_ref[n_pair * spots[b] + i, h * hd : (h + 1) * hd, :] = o[
                     16:, b * rows : (b + 1) * rows
                 ].astype(BF16)
             top = later
@@ -127,7 +127,7 @@
         hi = total.astype(BF16).astype(F32)
         stats = jnp.concatenate(tops + [hi, total - hi, jnp.zeros_like(total)], axis=0).astype(BF16)
         for b in range(2):
-            out_ref[2 * i + spots[b], qc:, :] = stats[:, b * rows : (b + 1) * rows]
+            out_ref[n_pair * spots[b] + i, qc:, :] = stats[:, b * rows : (b + 1) * rows]
         return top
 
     lax.fori_loop(0, n_pair, pair, score(0, 0, 0))
@@ -220,7 +220,7 @@
         ),
     )(lax.axis_index("zp").astype(jnp.int32)[None], query, kv)
     got = lax.all_to_all(
-        part, ("y", "zp"), 0, 0, tiled=True, axis_index_groups=[[2 * y + p for y in Y_ORDER for p in range(2)]]
+        part, ("y", "zp"), 0, 0, tiled=True, axis_index_groups=[[2 * y + p for p in range(2) for y in Y_ORDER]]
     )
 
     partial = call(

time: 88.3 us -> 88.4 us (level)
  no operation moved by 1% of the time
where the time goes in v10:
time: 88.4 us; the launch traced here: 88 us
  blocking collectives  55.7 us (63%)
  starting transfers between devices  14.6 us (17%)
  waiting for transfers between devices  9.15 us (10%)
  Pallas kernels  6.81 us (8%)
  other arithmetic  0.92 us (1%)
    all_to_all x1, blocking collectives, body(): lax.all_to_all(partial, TP, 0, 0, tiled=True, axis_index_groups=led_by(OU...  15.1 us
    all_to_all x1, blocking collectives, body(): lax.all_to_all(part, ('y', 'zp'), 0, 0, tiled=True, axis_index_groups=[[2...  13.3 us
    all_to_all x1, starting transfers between devices, body(): lax.all_to_all(kv, 'zq', 0, 0, tiled=True, axis_index_groups=led_by(Z_LEA...  12 us
    all_gather x1, blocking collectives, body(): lax.all_gather(jnp.stack([query, other]), 'y', axis=0, tiled=True, axis_i...  10.4 us
    ppermute x1, waiting for transfers between devices, body(): other = lax.ppermute(query, 'zp', [(0, 1), (1, 0)])  9.15 us
    all_to_all x1, blocking collectives, body(): lax.all_to_all(sent, 'x', 0, 0, tiled=True, axis_index_groups=[[(X_LEAD -...  8.79 us
    all_gather x1, blocking collectives, body(): lax.all_gather(tokens, 'c', axis=0, axis_index_groups=led_by(C_LEAD, n_c))  8.07 us
    pallas_call x1, Pallas kernels, body(): pl.pallas_call(functools.partial(attend_kernel, hd), out_shape=jax.ShapeD...  4.74 us
  transfers between devices with their start and end apart: 2, of which 1 were waited for; matrix products, arithmetic and copies ran while one was open for 0% of the time, Pallas kernels for 0%

profile of v10, /device:TPU:1, one launch (start us, length us, event | category | flops | bytes accessed | tf_op | source)
XLA Modules:
  0.0 88.0 jit_solution(14560819951192618297)
XLA Ops:
  0.0 0.0 copy-start.5
  0.0 0.0 copy-start.6
  0.0 0.0 copy-start.4
  0.1 0.6 copy-done.5
  0.7 0.0 copy-done.6
  0.7 0.1 multiply_cosine_fusion
  0.9 0.0 copy-done.4
  0.9 8.8 %all_to_all.20 = bf16[4,16,2048]{2,1,0:T(8,128)(2,1)S(1)} all-to-all(bf16[4,16,2048]{2,1,0:T(8,128)(2,1)S(1)} %broadcast_in_dim.5), channel_id=1, replica_groups={{4,2,0,6},{5,3,1,7},{12,10,8,14},{13,11,9,15},{20,18,16,22},{21,19,17,2..., dimensions={0} | all-to-all | bytes 524288 | tf_op jit(solution)/shard_map/all_to_all | solution.py:183
  9.7 8.1 %all-gather = bf16[8,16,2048]{2,1,0:T(8,128)(2,1)S(1)} all-gather(bf16[4,16,2048]{2,1,0:T(8,128)(2,1)S(1)} %all_to_all.20), channel_id=2, replica_groups={{1,0},{3,2},{5,4},{7,6},{9,8},{11,10},{13,12},{15,14},{17,16},{19,18},{..., dimensions={0}, use_global_device_ids=true | all-gather | bytes 786432 | tf_op jit(solution)/shard_map/all_gather | solution.py:184
  17.8 0.0 copy-done.2
  17.8 1.2 %shard_map.74 = bf16[8,128,128]{2,1,0:T(8,128)(2,1)} custom-call(bf16[128,2048]{1,0:T(8,128)(2,1)S(1)} %bitcast.9, bf16[64,2048]{1,0:T(8,128)(2,1)S(1)} %bitcast.14, bf16[64,2048]{1,0:T(8,128)(2,1)S(1)} %bitcast.15, f32[2,64]{1,0:T(2,128)S(1)} %pad_maximum_fusion.2.gain_ref, f32[4,16,128]{2,1,0:T(8,128)S(1)} %bitcast.11), custom_call_target="tpu_custom_call" | custom-call | flops 67108864 | bytes 1048576 | tf_op jit(solution)/shard_map/pallas_call | solution.py:194
  19.0 12.0 %all-to-all-start.1 = ((bf16[8,128,128]{2,1,0:T(8,128)(2,1)}), bf16[8,128,128]{2,1,0:T(8,128)(2,1)S(1)}, u32[]{:S(2)}, u32[]{:S(2)}) async-start(bf16[8,128,128]{2,1,0:T(8,128)(2,1)} %shard_map.74), calls=%async_computation.1 | async-start | bytes 524288 | tf_op jit(solution)/shard_map/all_to_all | solution.py:201
  31.0 0.0 copy-done
  31.0 0.4 shard_map.73
  31.4 2.6 %collective-permute-start = (bf16[256,128]{1,0:T(8,128)(2,1)S(1)}, bf16[256,128]{1,0:T(8,128)(2,1)S(1)}, u32[]{:S(2)}, u32[]{:S(2)}) collective-permute-start(bf16[256,128]{1,0:T(8,128)(2,1)S(1)} %shard_map.73), channel_id=1, source_target_pairs={{0,32},{32,0},{1,33},{33,1},{2,34},{34,2},{3,35},{35,3},{4,36},{36... | collective-permute-start | bytes 196616 | tf_op jit(solution)/shard_map/ppermute | solution.py:193
  34.1 9.1 %collective-permute-done = bf16[256,128]{1,0:T(8,128)(2,1)S(1)} collective-permute-done((bf16[256,128]{1,0:T(8,128)(2,1)S(1)}, bf16[256,128]{1,0:T(8,128)(2,1)S(1)}, u32[]{:S(2)}, u32[]{:S(2)}) %collective-permute-start) | collective-permute-done | bytes 65568 | tf_op jit(solution)/shard_map/ppermute | solution.py:193
  43.2 10.4 %all_gather.11.q_ref = bf16[8,256,128]{2,1,0:T(8,128)(2,1)S(1)} all-gather(bf16[2,256,128]{2,1,0:T(8,128)(2,1)S(1)} %pad_maximum_fusion), channel_id=1, replica_groups={{16,8,0,24},{17,9,1,25},{18,10,2,26},{19,11,3,27},{20,12,4,28},{21,13,5..., dimensions={0}, use_global_device_ids=true | all-gather | bytes 655360 | tf_op jit(solution)/shard_map/all_gather | solution.py:202
  53.6 0.0 all-to-all-done.1.kv_ref
  53.6 4.7 %shard_map.75 = bf16[8,272,128]{2,1,0:T(8,128)(2,1)S(1)} custom-call(s32[1]{0:T(128)} %bitcast.zp_ref, bf16[8,256,128]{2,1,0:T(8,128)(2,1)S(1)} %all_gather.11.q_ref, bf16[8,128,128]{2,1,0:T(8,128)(2,1)S(1)} %all-to-all-done.1.kv_ref), custom_call_target="tpu_custom_call" | custom-call | flops 1073741824 | bytes 1048576 | tf_op jit(solution)/shard_map/pallas_call | solution.py:205
  58.4 0.0 copy-start.1
  58.4 13.3 %all_to_all.21.got_ref = bf16[8,272,128]{2,1,0:T(8,128)(2,1)S(1)} all-to-all(bf16[8,272,128]{2,1,0:T(8,128)(2,1)S(1)} %shard_map.75), channel_id=1, replica_groups={{16,8,0,24,48,40,32,56},{17,9,1,25,49,41,33,57},{18,10,2,26,50,42,34,58..., dimensions={0} | all-to-all | bytes 1114112 | tf_op jit(solution)/shard_map/all_to_all | solution.py:222
  71.7 0.4 shard_map.76
  72.2 15.1 %all_to_all.22 = bf16[8,16,2048]{2,1,0:T(8,128)(2,1)S(1)} all-to-all(bf16[8,16,2048]{2,1,0:T(8,128)(2,1)S(1)} %shard_map.76), channel_id=1, replica_groups={{5,6,7,0,1,2,3,4},{13,14,15,8,9,10,11,12},{21,22,23,16,17,18,19,20},{29..., dimensions={0} | all-to-all | bytes 1048576 | tf_op jit(solution)/shard_map/all_to_all | solution.py:234
  87.3 0.7 reduce_sum.12
  (12 shorter events, 0.1 us)
Async XLA Ops:
  0.0 0.7 copy-start.5
  0.0 0.7 copy-start.6
  0.0 0.8 copy-start.4
  9.7 8.1 %copy-start.2 = (bf16[2048,64]{0,1:T(8,128)(2,1)S(1)}, bf16[2048,64]{0,1:T(8,128)(2,1)}, u32[]{:S(2)}) copy-start(bf16[2048,64]{0,1:T(8,128)(2,1)} %param.9) | copy-start | bytes 786436
  9.7 8.1 %copy-start.3 = (bf16[2048,64]{0,1:T(8,128)(2,1)S(1)}, bf16[2048,64]{0,1:T(8,128)(2,1)}, u32[]{:S(2)}) copy-start(bf16[2048,64]{0,1:T(8,128)(2,1)} %param.10) | copy-start | bytes 786436
  17.8 13.2 %copy-start = (bf16[2048,256]{1,0:T(8,128)(2,1)S(1)}, bf16[2048,256]{1,0:T(8,128)(2,1)}, u32[]{:S(2)}) copy-start(bf16[2048,256]{1,0:T(8,128)(2,1)} %w_ref.2) | copy-start | bytes 3145732
  19.0 34.6 %all-to-all-start.1 = ((bf16[8,128,128]{2,1,0:T(8,128)(2,1)}), bf16[8,128,128]{2,1,0:T(8,128)(2,1)S(1)}, u32[]{:S(2)}, u32[]{:S(2)}) async-start(bf16[8,128,128]{2,1,0:T(8,128)(2,1)} %shard_map.74), calls=%async_computation.1 | async-start | bytes 524288 | tf_op jit(solution)/shard_map/all_to_all | solution.py:201
  31.4 11.8 %collective-permute-start = (bf16[256,128]{1,0:T(8,128)(2,1)S(1)}, bf16[256,128]{1,0:T(8,128)(2,1)S(1)}, u32[]{:S(2)}, u32[]{:S(2)}) collective-permute-start(bf16[256,128]{1,0:T(8,128)(2,1)S(1)} %shard_map.73), channel_id=1, source_target_pairs={{0,32},{32,0},{1,33},{33,1},{2,34},{34,2},{3,35},{35,3},{4,36},{36... | collective-permute-start | bytes 196616 | tf_op jit(solution)/shard_map/ppermute | solution.py:193
  58.4 13.3 %copy-start.1 = (bf16[256,2048]{1,0:T(8,128)(2,1)S(1)}, bf16[256,2048]{1,0:T(8,128)(2,1)}, u32[]{:S(2)}) copy-start(bf16[256,2048]{1,0:T(8,128)(2,1)} %w_ref.3) | copy-start | bytes 3145732
